TPU v7x, 256 devices: a 4x2x16 block of a 4x16x16 slice. The times are simulated.
256 devices in a mesh: grp: 2 (over y), fs: 16 (over z), tp: 8 (over x, core).
Axes of the slice: x: 4, y: 2, z: 16, core: 2. Of those that a mesh axis runs over, the one named last changes fastest.
The devices are a block of a 4x16x16 slice.
Arguments:
- tokens: bfloat16 [32, 1024, 2048], P(('grp', 'fs'), None, 'tp'), parts along dimension 0, may hold values from -6 to 6
- mix_gain: float32 [2048], replicated, may hold values from 0.1 to 1.9
- in_matrix: float32 [2048, 1024], P('fs', 'tp'), may hold values from -0.125 to 0.125
- in_scale: float32 [1, 1024], P(None, 'tp'), may hold values from 0.5 to 2
- pool_mix: bfloat16 [8, 128, 128], P('tp'), may hold values from -0.5 to 0.5
- pool_scale: float32 [1, 1024], P(None, 'tp'), may hold values from 0.1 to 1.9
- out_matrix: float32 [1024, 2048], P('tp', 'fs'), may hold values from -0.25 to 0.25
- out_scale: float32 [1, 2048], P(None, 'fs'), may hold values from 0.5 to 2
- ffn_gain: float32 [2048], replicated, may hold values from 0.1 to 1.9
- gate_matrix: float32 [2048, 5632], P('fs', 'tp'), may hold values from -0.125 to 0.125
- gate_scale: float32 [1, 5632], P(None, 'tp'), may hold values from 0.5 to 2
- up_matrix: float32 [2048, 5632], P('fs', 'tp'), may hold values from -0.125 to 0.125
- up_scale: float32 [1, 5632], P(None, 'tp'), may hold values from 0.5 to 2
- gate_taps: float32 [3, 5632], P(None, 'tp'), may hold values from -4 to 4
- up_taps: float32 [3, 5632], P(None, 'tp'), may hold values from -4 to 4
- down_matrix: float32 [5632, 2048], P('tp', 'fs'), may hold values from -0.109375 to 0.109375
- down_scale: float32 [1, 2048], P(None, 'fs'), may hold values from 0.5 to 2
Outputs:
- layer_out: bfloat16 [32, 1024, 2048], P(('grp', 'fs'), None, 'tp'), parts along dimension 0
There are 2 independent parts, one for each index of `grp`. A program takes and returns all parts, laid end to end along the dimension named above; an argument that names none is the same for every part. Nothing has to cross between parts.
All inputs are finite; a program needn't handle non-finite values.
Results may differ from a plain program's by a relative error of at most 0.025.
Values may be sent and summed in bfloat16 or wider, within the bound.
A program may use at most 64 MiB of HBM per device.

v0:
```python
import jax
import jax.numpy as jnp
from jax import lax
from jax.sharding import PartitionSpec as P

BLOCKS = 8


eps = 1e-06
widest_span = 16


def sent_together(arrays, axis, dim, along):
    ends, at = ([], 0)
    for a in arrays[:-1]:
        at += a.shape[along]
        ends.append(at)
    both = jnp.concatenate(arrays, axis=along)
    return tuple(jnp.split(lax.all_gather(both, axis, axis=dim, tiled=True), ends, axis=along))


def in_order(blocks, dim):
    lengths = list(blocks.shape[1:])
    lengths[dim] *= blocks.shape[0]
    return jnp.moveaxis(blocks, 0, dim).reshape(lengths)


def from_everyone(x, axis):
    copies = jnp.broadcast_to(x, (lax.axis_size(axis), *x.shape))
    return lax.all_to_all(copies, axis, split_axis=0, concat_axis=0, tiled=True)


def collect(x, axis, dim):
    return in_order(from_everyone(x, axis), dim)


def norm_rows(tok_rows, norm_gain):
    values = tok_rows.astype(jnp.float32)
    scaled = values * lax.rsqrt(jnp.mean(values * values, axis=-1, keepdims=True) + eps)
    return (scaled * norm_gain).astype(jnp.bfloat16)


def span_widths(block_ids):
    return jnp.left_shift(jnp.ones_like(block_ids), 1 + 4 * block_ids // BLOCKS)


def trailing_gap(projected, windows):
    values = projected.astype(jnp.float32)
    length = values.shape[0]
    running = values
    for offset in range(1, widest_span):
        shifted = jnp.pad(values[: length - offset], ((offset, 0), (0, 0)))
        running = running + jnp.where(windows[None, :] > offset, shifted, jnp.zeros_like(shifted))
    positions = jnp.arange(length, dtype=jnp.int32)[:, None]
    counts = jnp.minimum(positions + 1, windows[None, :]).astype(jnp.float32)
    return (running / counts - values).astype(jnp.bfloat16)


def causal_taps(linear, tap_table):
    values = linear.astype(jnp.float32)
    length = values.shape[0]
    back_one = jnp.pad(values[: length - 1], ((1, 0), (0, 0)))
    back_two = jnp.pad(values[: length - 2], ((2, 0), (0, 0)))
    return tap_table[2] * values + tap_table[1] * back_one + tap_table[0] * back_two


def fold_rows(operand, portion):
    return jnp.dot(operand, portion, preferred_element_type=jnp.float32)


def shards(
    tokens,
    mix_gain,
    in_matrix,
    in_scale,
    pool_mix,
    pool_scale,
    out_matrix,
    out_scale,
    ffn_gain,
    gate_matrix,
    gate_scale,
    up_matrix,
    up_scale,
    gate_taps,
    up_taps,
    down_matrix,
    down_scale,
):
    length = tokens.shape[1]
    own_width = tokens.shape[2]
    local_rows = tokens.reshape(length, own_width)
    out_cols, down_cols = sent_together((out_scale, down_scale), "fs", 1, 0)
    gathered = collect(local_rows, "tp", 1)
    normed = norm_rows(gathered, mix_gain)
    width_in = in_matrix.shape[1]
    in_total = fold_rows(normed, collect(in_matrix.astype(jnp.bfloat16), "fs", 0))
    projected = (in_total * in_scale).astype(jnp.bfloat16)
    local_blocks = pool_mix.shape[0]
    block_width = pool_mix.shape[1]
    block_ids = lax.axis_index("tp") * local_blocks + jnp.arange(local_blocks, dtype=jnp.int32)
    windows = jnp.repeat(span_widths(block_ids), block_width)
    spread = trailing_gap(projected, windows)
    block_mixed = jnp.einsum(
        "lbc,bce->lbe",
        spread.reshape(length, local_blocks, block_width),
        pool_mix,
        preferred_element_type=jnp.float32,
    ).reshape(length, width_in)
    pooled = (block_mixed * pool_scale).astype(jnp.bfloat16)
    tp_index = lax.axis_index("tp")
    groups = lax.axis_size("tp")
    pooled_all = collect(pooled, "tp", 1)
    row_block = collect(out_matrix.astype(jnp.bfloat16), "fs", 1)
    own_matrix = lax.all_to_all(row_block, "tp", split_axis=1, concat_axis=0, tiled=True)
    own_scales = lax.dynamic_slice_in_dim(out_cols, tp_index * own_width, own_width, 1)
    grouped_rows = pooled_all.reshape(length, groups, width_in)
    grouped_matrix = own_matrix.reshape(groups, width_in, own_width)
    pieces = (
        jnp.einsum("lgc,gcd->gld", grouped_rows, grouped_matrix, preferred_element_type=jnp.float32)
        * own_scales[None]
    )
    rounded = lax.optimization_barrier(pieces.astype(jnp.bfloat16))
    mixing = jnp.sum(rounded.astype(jnp.float32), axis=0)
    residual = (local_rows.astype(jnp.float32) + mixing).astype(jnp.bfloat16)
    gathered_ffn = collect(residual, "tp", 1)
    normed_ffn = norm_rows(gathered_ffn, ffn_gain)
    gate_cast = gate_matrix.astype(jnp.bfloat16)
    up_cast = up_matrix.astype(jnp.bfloat16)
    gate_full, up_full = sent_together((gate_cast, up_cast), "fs", 0, 1)
    gate_total = jnp.dot(normed_ffn, gate_full, preferred_element_type=jnp.float32)
    up_total = jnp.dot(normed_ffn, up_full, preferred_element_type=jnp.float32)
    gate_lin = (gate_total * gate_scale).astype(jnp.bfloat16)
    up_lin = (up_total * up_scale).astype(jnp.bfloat16)
    hidden = (jax.nn.silu(causal_taps(gate_lin, gate_taps)) * causal_taps(up_lin, up_taps)).astype(
        jnp.bfloat16
    )
    partial_ffn = (
        jnp.dot(
            hidden,
            lax.all_gather(down_matrix.astype(jnp.bfloat16), "fs", axis=1, tiled=True),
            preferred_element_type=jnp.float32,
        )
        * down_cols
    )
    feed_out = lax.psum_scatter(
        partial_ffn.astype(jnp.bfloat16), "tp", scatter_dimension=1, tiled=True
    ).astype(jnp.float32)
    result = (residual.astype(jnp.float32) + feed_out).astype(jnp.bfloat16)
    return result.reshape(1, length, result.shape[1])


def solution(mesh):
    return jax.shard_map(
        shards,
        mesh=mesh,
        in_specs=(
            P(("grp", "fs"), None, "tp"),
            P(),
            P("fs", "tp"),
            P(None, "tp"),
            P("tp", None, None),
            P(None, "tp"),
            P("tp", "fs"),
            P(None, "fs"),
            P(),
            P("fs", "tp"),
            P(None, "tp"),
            P("fs", "tp"),
            P(None, "tp"),
            P(None, "tp"),
            P(None, "tp"),
            P("tp", "fs"),
            P(None, "fs"),
        ),
        out_specs=P(("grp", "fs"), None, "tp"),
        check_vma=False,
    )
```

profile of v0, /device:TPU:33, one launch (start us, length us, event | category | flops | bytes accessed | tf_op | source)
XLA Modules:
  0.0 362.5 jit_solution(4619885628896083093)
XLA Ops:
  6.5 0.0 copy-start
  6.6 0.9 convert_element_type.148
  7.5 0.1 copy.19
  7.6 0.9 broadcast_in_dim.121
  8.5 24.5 %all-to-all-start.3 = ((bf16[16,128,128]{1,2,0:T(8,128)(2,1)}), bf16[16,128,128]{1,2,0:T(8,128)(2,1)S(1)}, u32[]{:S(2)}, u32[]{:S(2)}) async-start(bf16[16,128,128]{1,2,0:T(8,128)(2,1)} %broadcast_in_dim.121), calls=%async_computation.3 | async-start | bytes 1048576 | tf_op jit(solution)/shard_map/all_to_all | solution.py:30
  33.0 0.1 all-gather.3.cloned.1.call-start
  33.1 1.0 convert_element_type.158
  34.1 1.0 convert_element_type.159
  35.1 0.8 pad_maximum_fusion
  35.9 0.1 all-gather.3.cloned.1.call-update
  35.9 0.0 copy-done.2
  35.9 0.2 copy.18
  36.1 19.6 %all-to-all-done.3 = bf16[16,128,128]{1,2,0:T(8,128)(2,1)S(1)} async-done(((bf16[16,128,128]{1,2,0:T(8,128)(2,1)}), bf16[16,128,128]{1,2,0:T(8,128)(2,1)S(1)}, u32[]{:S(2)}, u32[]{:S(2)}) %all-to-all-start.3) | async-done | bytes 524320 | tf_op jit(solution)/shard_map/all_to_all | solution.py:30
  55.8 2.6 broadcast_in_dim.102
  58.4 11.7 %all-to-all-start = ((bf16[8,1024,256]{1,2,0:T(8,128)(2,1)}), bf16[8,1024,256]{1,2,0:T(8,128)(2,1)}, u32[]{:S(2)}, u32[]{:S(2)}) async-start(bf16[8,1024,256]{1,2,0:T(8,128)(2,1)} %broadcast_in_dim.102), calls=%async_computation | async-start | bytes 8388608 | tf_op jit(solution)/shard_map/all_to_all | solution.py:30
  70.1 0.0 copy-done.4
  70.1 48.8 %all-to-all-done = bf16[8,1024,256]{1,2,0:T(8,128)(2,1)} async-done(((bf16[8,1024,256]{1,2,0:T(8,128)(2,1)}), bf16[8,1024,256]{1,2,0:T(8,128)(2,1)}, u32[]{:S(2)}, u32[]{:S(2)}) %all-to-all-start) | async-done | bytes 4194336 | tf_op jit(solution)/shard_map/all_to_all | solution.py:30
  118.9 0.9 broadcast_in_dim.103
  119.8 7.9 %all-to-all-start.1 = ((bf16[16,128,128]{2,1,0:T(8,128)(2,1)}), bf16[16,128,128]{2,1,0:T(8,128)(2,1)S(1)}, u32[]{:S(2)}, u32[]{:S(2)}) async-start(bf16[16,128,128]{2,1,0:T(8,128)(2,1)} %broadcast_in_dim.103), calls=%async_computation.1 | async-start | bytes 1048576 | tf_op jit(solution)/shard_map/all_to_all | solution.py:30
  127.8 0.0 copy-done.6
  127.8 1.0 copy.20
  128.8 3.1 fusion
  131.9 0.0 copy-start.14
  131.9 4.3 %fusion.2 = bf16[8,1024,256]{1,2,0:T(8,128)(2,1)} fusion(bf16[8,1024,256]{1,2,0:T(8,128)(2,1)} %all-to-all-done, f32[8,256]{1,0:T(8,128)S(1)} %mul.187, f32[1024]{0:T(1024)S(1)} %add_rsqrt_fusion.1), kind=kLoop, calls=%fused_computation.4 | loop fusion | flops 8388608 | bytes 8400896 | tf_op jit(solution)/shard_map/convert_element_type | solution.py:40
  136.2 20.4 %all-to-all-done.1 = bf16[16,128,128]{2,1,0:T(8,128)(2,1)S(1)} async-done(((bf16[16,128,128]{2,1,0:T(8,128)(2,1)}), bf16[16,128,128]{2,1,0:T(8,128)(2,1)S(1)}, u32[]{:S(2)}, u32[]{:S(2)}) %all-to-all-start.1) | async-done | bytes 524320 | tf_op jit(solution)/shard_map/all_to_all | solution.py:30
  156.6 9.8 %all-to-all-start.4 = ((bf16[128,8,256]{2,0,1:T(8,128)(2,1)}), bf16[128,8,256]{2,0,1:T(8,128)(2,1)S(1)}, u32[]{:S(2)}, u32[]{:S(2)}) async-start(bf16[128,8,256]{2,0,1:T(8,128)(2,1)} %copy.20), calls=%async_computation.4 | async-start | bytes 1048576 | tf_op jit(solution)/shard_map/all_to_all | solution.py:115
  166.4 0.0 copy-done.14
  166.4 3.5 fusion.22
  170.0 0.0 copy-start.15
  170.2 0.0 copy-done
  170.3 0.4 copy-done.15
  170.6 1.5 fusion.20
  172.2 3.6 all-to-all-done.4
  175.8 1.6 broadcast_in_dim.120
  177.4 4.5 %all-to-all-start.2 = ((bf16[8,1024,128]{2,1,0:T(8,128)(2,1)}), bf16[8,1024,128]{2,1,0:T(8,128)(2,1)S(1)}, u32[]{:S(2)}, u32[]{:S(2)}) async-start(bf16[8,1024,128]{2,1,0:T(8,128)(2,1)} %broadcast_in_dim.120), calls=%async_computation.2 | async-start | bytes 4194304 | tf_op jit(solution)/shard_map/all_to_all | solution.py:30
  181.8 0.0 copy-done.11
  181.8 0.0 copy-done.12
  181.9 20.3 %all_gather.9 = f32[2,2048]{1,0:T(2,128)S(1)} all-gather(f32[2,128]{1,0:T(2,128)S(1)} %pad_maximum_fusion.1), channel_id=1, replica_groups=mesh['grp'=2,'fs'=16,'tp'=8] {'fs'}, dimensions={1}, use_global_device_ids=true | all-gather | bytes 17408 | tf_op jit(solution)/shard_map/all_gather | solution.py:19
  202.2 5.9 %all-to-all-done.2 = bf16[8,1024,128]{2,1,0:T(8,128)(2,1)S(1)} async-done(((bf16[8,1024,128]{2,1,0:T(8,128)(2,1)}), bf16[8,1024,128]{2,1,0:T(8,128)(2,1)S(1)}, u32[]{:S(2)}, u32[]{:S(2)}) %all-to-all-start.2) | async-done | bytes 2097184 | tf_op jit(solution)/shard_map/all_to_all | solution.py:30
  208.1 1.2 multiply_convert_fusion.1
  209.4 0.6 convert_reduce_fusion
  210.0 0.1 add_convert_fusion.1
  210.1 0.2 copy.21
  210.3 2.6 broadcast_in_dim.122
  212.9 0.0 copy-start.8
  213.0 5.5 %all-to-all-start.5 = ((bf16[8,1024,256]{1,2,0:T(8,128)(2,1)}), bf16[8,1024,256]{1,2,0:T(8,128)(2,1)}, u32[]{:S(2)}, u32[]{:S(2)}) async-start(bf16[8,1024,256]{1,2,0:T(8,128)(2,1)} %broadcast_in_dim.122), calls=%async_computation.5 | async-start | bytes 8388608 | tf_op jit(solution)/shard_map/all_to_all | solution.py:30
  218.5 0.0 all-gather.5.cloned.1.call-start
  218.5 0.0 copy-done.3
  218.5 0.7 convert_element_type.165
  219.2 0.1 all-gather.5.cloned.1.call-update
  219.3 0.2 reduce-scatter.2.cloned.1.call-start
  219.5 0.0 copy-done.9
  219.6 0.1 slice_reduce_fusion.2
  219.7 47.7 %all-to-all-done.5 = bf16[8,1024,256]{1,2,0:T(8,128)(2,1)} async-done(((bf16[8,1024,256]{1,2,0:T(8,128)(2,1)}), bf16[8,1024,256]{1,2,0:T(8,128)(2,1)}, u32[]{:S(2)}, u32[]{:S(2)}) %all-to-all-start.5) | async-done | bytes 4194336 | tf_op jit(solution)/shard_map/all_to_all | solution.py:30
  267.4 3.1 multiply_reduce_fusion
  270.5 4.2 %fusion.4 = bf16[1024,2048]{0,1:T(8,128)(2,1)} fusion(f32[2048]{0:T(1024)S(1)} %copy-done.5, f32[1024]{0:T(1024)S(1)} %add_rsqrt_fusion, bf16[8,1024,256]{1,2,0:T(8,128)(2,1)} %all-to-all-done.5), kind=kLoop, calls=%fused_computation.7 | loop fusion | flops 8388608 | bytes 8400896 | tf_op jit(solution)/shard_map/convert_element_type | solution.py:40
  274.7 8.0 %fusion.17 = f32[1024,704]{0,1:T(8,128)} fusion(bf16[1024,2048]{0,1:T(8,128)(2,1)} %fusion.4, bf16[2048,1408]{0,1:T(8,128)(2,1)} %all-gather.3.cloned.1.call-done, f32[704]{0:T(1024)S(1)} %reduce.9), kind=kOutput, calls=%fused_computation.21 | convolution fusion | flops 2954952704 | bytes 9964288 | tf_op jit(solution)/shard_map/dot_general | solution.py:132
  282.7 0.0 copy-done.13
  282.7 4.8 %fusion.14 = f32[1024,704]{0,1:T(8,128)} fusion(bf16[1024,2048]{0,1:T(8,128)(2,1)S(1)} %copy-done.1, bf16[2048,1408]{0,1:T(8,128)(2,1)S(1)} %copy-done.13, f32[704]{0:T(1024)S(1)} %reduce.5), kind=kOutput, calls=%fused_computation.20 | convolution fusion | flops 2954952704 | bytes 9965568 | tf_op jit(solution)/shard_map/dot_general | solution.py:131
  287.6 3.1 all-gather.5.cloned.1.call-done
  290.6 15.5 %multiply_convert_fusion = bf16[1024,2048]{1,0:T(8,128)(2,1)} fusion(bf16[704,2048]{1,0:T(8,128)(2,1)} %all-gather.5.cloned.1.call-done, f32[2048]{0:T(1024)S(1)} %bitcast.76, f32[1022,704]{0,1:T(8,128)} %bitcast.80, f32[1023,704]{0,1:T(8,128)} %bitcast.81, f32[1024,704]{0,1:T(8,128)} %fusion.17, f32[1022,704]{0,1:T(8,128)} %bitcast.82, ...), kind=kOutput, calls=%fused_computation.8 | convolution fusion | flops 2968518656 | bytes 24387584 | tf_op jit(solution)/shard_map/dot_general | solution.py:139
  306.2 0.1 reduce-scatter.2.cloned.1.call-update
  306.2 47.7 %reduce-scatter.2.cloned.1.call-done = bf16[1024,256]{1,0:T(8,128)(2,1)} async-done(((bf16[1024,2048]{1,0:T(8,128)(2,1)}), bf16[1024,256]{1,0:T(8,128)(2,1)}) %reduce-scatter.2.cloned.1.call-update) | async-done | bytes 524304 | tf_op jit(solution)/shard_map/reduce_scatter | solution.py:146
  354.0 2.0 fusion.23
  (36 shorter events, 0.4 us)
Async XLA Ops:
  6.5 163.7 %copy-start = (bf16[1,128,128]{2,1,0:T(8,128)(2,1)S(1)}, bf16[1,128,128]{2,1,0:T(8,128)(2,1)}, u32[]{:S(2)}) copy-start(bf16[1,128,128]{2,1,0:T(8,128)(2,1)} %param.21) | copy-start | bytes 98308
  6.6 29.4 %copy-start.2 = (bf16[1,1024,256]{2,1,0:T(8,128)(2,1)S(1)}, bf16[1,1024,256]{2,1,0:T(8,128)(2,1)}, u32[]{:S(2)}) copy-start(bf16[1,1024,256]{2,1,0:T(8,128)(2,1)} %param.17) | copy-start | bytes 1572868
  8.5 47.3 %all-to-all-start.3 = ((bf16[16,128,128]{1,2,0:T(8,128)(2,1)}), bf16[16,128,128]{1,2,0:T(8,128)(2,1)S(1)}, u32[]{:S(2)}, u32[]{:S(2)}) async-start(bf16[16,128,128]{1,2,0:T(8,128)(2,1)} %broadcast_in_dim.121), calls=%async_computation.3 | async-start | bytes 1048576 | tf_op jit(solution)/shard_map/all_to_all | solution.py:30
  33.0 241.7 %all-gather.3.cloned.1.call-start = ((), (), s32[]{:S(2)}) async-start(), calls=%async_computation.7 | async-start | bytes 6127616 | tf_op jit(solution)/shard_map/all_gather | solution.py:19
  58.4 11.8 %copy-start.4 = (f32[128,128]{1,0:T(8,128)S(1)}, f32[128,128]{1,0:T(8,128)}, u32[]{:S(2)}) copy-start(f32[128,128]{1,0:T(8,128)} %param.19) | copy-start | bytes 196612
  58.4 69.4 %copy-start.6 = (f32[2048]{0:T(1024)S(1)}, f32[2048]{0:T(1024)}, u32[]{:S(2)}) copy-start(f32[2048]{0:T(1024)} %param.18) | copy-start | bytes 24580
  58.4 60.5 %all-to-all-start = ((bf16[8,1024,256]{1,2,0:T(8,128)(2,1)}), bf16[8,1024,256]{1,2,0:T(8,128)(2,1)}, u32[]{:S(2)}, u32[]{:S(2)}) async-start(bf16[8,1024,256]{1,2,0:T(8,128)(2,1)} %broadcast_in_dim.102), calls=%async_computation | async-start | bytes 8388608 | tf_op jit(solution)/shard_map/all_to_all | solution.py:30
  119.8 36.8 %all-to-all-start.1 = ((bf16[16,128,128]{2,1,0:T(8,128)(2,1)}), bf16[16,128,128]{2,1,0:T(8,128)(2,1)S(1)}, u32[]{:S(2)}, u32[]{:S(2)}) async-start(bf16[16,128,128]{2,1,0:T(8,128)(2,1)} %broadcast_in_dim.103), calls=%async_computation.1 | async-start | bytes 1048576 | tf_op jit(solution)/shard_map/all_to_all | solution.py:30
  131.9 34.5 %copy-start.14 = (f32[1,128]{1,0:T(1,128)S(1)}, f32[1,128]{1,0:T(1,128)}, u32[]{:S(2)}) copy-start(f32[1,128]{1,0:T(1,128)} %param.20) | copy-start | bytes 1540
  156.6 19.2 %all-to-all-start.4 = ((bf16[128,8,256]{2,0,1:T(8,128)(2,1)}), bf16[128,8,256]{2,0,1:T(8,128)(2,1)S(1)}, u32[]{:S(2)}, u32[]{:S(2)}) async-start(bf16[128,8,256]{2,0,1:T(8,128)(2,1)} %copy.20), calls=%async_computation.4 | async-start | bytes 1048576 | tf_op jit(solution)/shard_map/all_to_all | solution.py:115
  170.0 0.7 copy-start.15
  172.2 9.7 %copy-start.11 = (f32[1,128]{1,0:T(1,128)S(1)}, f32[1,128]{1,0:T(1,128)}, u32[]{:S(2)}) copy-start(f32[1,128]{1,0:T(1,128)} %param.33) | copy-start | bytes 1540
  172.2 9.7 %copy-start.12 = (f32[1,128]{1,0:T(1,128)S(1)}, f32[1,128]{1,0:T(1,128)}, u32[]{:S(2)}) copy-start(f32[1,128]{1,0:T(1,128)} %param.24) | copy-start | bytes 1540
  177.4 30.8 %all-to-all-start.2 = ((bf16[8,1024,128]{2,1,0:T(8,128)(2,1)}), bf16[8,1024,128]{2,1,0:T(8,128)(2,1)S(1)}, u32[]{:S(2)}, u32[]{:S(2)}) async-start(bf16[8,1024,128]{2,1,0:T(8,128)(2,1)} %broadcast_in_dim.120), calls=%async_computation.2 | async-start | bytes 4194304 | tf_op jit(solution)/shard_map/all_to_all | solution.py:30
  212.9 5.6 %copy-start.3 = (f32[704,128]{1,0:T(8,128)S(1)}, f32[704,128]{1,0:T(8,128)}, u32[]{:S(2)}) copy-start(f32[704,128]{1,0:T(8,128)} %param.32) | copy-start | bytes 1081348
  212.9 6.6 %copy-start.9 = (f32[1,704]{1,0:T(1,128)S(1)}, f32[1,704]{1,0:T(1,128)}, u32[]{:S(2)}) copy-start(f32[1,704]{1,0:T(1,128)} %param.29) | copy-start | bytes 8452
  212.9 6.6 %copy-start.10 = (f32[1,704]{1,0:T(1,128)S(1)}, f32[1,704]{1,0:T(1,128)}, u32[]{:S(2)}) copy-start(f32[1,704]{1,0:T(1,128)} %param.27) | copy-start | bytes 8452
  212.9 6.6 %copy-start.7 = (f32[3,704]{1,0:T(4,128)S(1)}, f32[3,704]{1,0:T(4,128)}, u32[]{:S(2)}) copy-start(f32[3,704]{1,0:T(4,128)} %param.31) | copy-start | bytes 25348
  212.9 6.6 %copy-start.8 = (f32[3,704]{1,0:T(4,128)S(1)}, f32[3,704]{1,0:T(4,128)}, u32[]{:S(2)}) copy-start(f32[3,704]{1,0:T(4,128)} %param.30) | copy-start | bytes 25348
  213.0 54.4 %all-to-all-start.5 = ((bf16[8,1024,256]{1,2,0:T(8,128)(2,1)}), bf16[8,1024,256]{1,2,0:T(8,128)(2,1)}, u32[]{:S(2)}, u32[]{:S(2)}) async-start(bf16[8,1024,256]{1,2,0:T(8,128)(2,1)} %broadcast_in_dim.122), calls=%async_computation.5 | async-start | bytes 8388608 | tf_op jit(solution)/shard_map/all_to_all | solution.py:30
  218.5 52.0 %copy-start.5 = (f32[2048]{0:T(1024)S(1)}, f32[2048]{0:T(1024)}, u32[]{:S(2)}) copy-start(f32[2048]{0:T(1024)} %param.25) | copy-start | bytes 24580
  218.5 72.1 %all-gather.5.cloned.1.call-start = ((), (), s32[]{:S(2)}) async-start(), calls=%async_computation.8 | async-start | bytes 3063808 | tf_op jit(solution)/shard_map/all_gather | solution.py:141
  219.3 134.7 %reduce-scatter.2.cloned.1.call-start = ((), (), s32[]{:S(2)}) async-start(), calls=%async_computation.9 | async-start | bytes 4718592 | tf_op jit(solution)/shard_map/reduce_scatter | solution.py:146
  274.7 8.0 %copy-start.1 = (bf16[1024,2048]{0,1:T(8,128)(2,1)S(1)}, bf16[1024,2048]{0,1:T(8,128)(2,1)}, u32[]{:S(2)}) copy-start(bf16[1024,2048]{0,1:T(8,128)(2,1)} %fusion.4) | copy-start | bytes 12582916
  274.7 8.0 %copy-start.13 = (bf16[2048,1408]{0,1:T(8,128)(2,1)S(1)}, bf16[2048,1408]{0,1:T(8,128)(2,1)}, u32[]{:S(2)}) copy-start(bf16[2048,1408]{0,1:T(8,128)(2,1)} %all-gather.3.cloned.1.call-done) | copy-start | bytes 17301508
Sparse Core Ops, SparseCore 0:
  36.0 120.0 all-gather.2
  221.0 69.5 all-gather.4
  306.3 47.5 reduce-scatter.1
where the time goes:
time: 364 us; the launch traced here: 362 us
  waiting for transfers between devices  197 us (54%)
  starting transfers between devices  64.3 us (18%)
  matrix products  34.6 us (10%)
  other arithmetic  21.8 us (6%)
  blocking collectives  20.3 us (6%)
  between operations  13.5 us (4%)
  local copies, waits for them, and re-layouts  11 us (3%)
    all_to_all x5, waiting for transfers between devices, from_everyone(): return lax.all_to_all(copies, axis, split_axis=0, concat_axis=0, tiled=True)  142 us
    all_to_all x5, starting transfers between devices, from_everyone(): return lax.all_to_all(copies, axis, split_axis=0, concat_axis=0, tiled=True)  54.2 us
    reduce_scatter x1, waiting for transfers between devices, shards(): lax.psum_scatter(partial_ffn.astype(jnp.bfloat16), 'tp', scatter_dimensio...  47.7 us
    all_gather x1, blocking collectives, sent_together(): lax.all_gather(both, axis, axis=dim, tiled=True)  20.3 us
    dot_general x1, matrix products, shards(): jnp.dot(hidden, lax.all_gather(down_matrix.astype(jnp.bfloat16), 'fs', ax...  15.5 us
    all_to_all x1, starting transfers between devices, shards(): lax.all_to_all(row_block, 'tp', split_axis=1, concat_axis=0, tiled=True)  9.83 us
    broadcast_in_dim x5, local copies, waits for them, and re-layouts, from_everyone(): copies = jnp.broadcast_to(x, (lax.axis_size(axis), *x.shape))  8.65 us
    convert_element_type x2, other arithmetic, norm_rows(): return (scaled * norm_gain).astype(jnp.bfloat16)  8.47 us
  transfers between devices with their start and end apart: 9, of which 8 were waited for; matrix products, arithmetic and copies ran while one was open for 13% of the time, Pallas kernels for 0%

commit v1 on v0

v1 whole, which is shorter than its diff:
```python
import functools

import jax
import jax.numpy as jnp
from jax import lax
from jax.experimental import pallas as pl
from jax.experimental.pallas import tpu as pltpu
from jax.sharding import PartitionSpec as P

MESH = pl.DeviceIdType.MESH
EPS = 1e-06
BF16 = jnp.bfloat16
F32 = jnp.float32
LANES = 128
CORES = 2


class FeatureGather:
    TAGS = 13
    R0, R1, L1, L0, F0, F1, OWN, PL0, PL1, PR0, PR1, PO0, PO1 = range(13)

    def __init__(self, buf, send, recv, chips, x, core):
        self.buf, self.send, self.recv = buf, send, recv
        self.half = buf.shape[1] // 2
        at = lambda chip, c: lax.rem(chip, chips) * CORES + c
        other = 1 - core
        self.me, self.mate = at(x, core), at(x, other)
        self.right, self.left, self.far = at(x + 1, core), at(x + chips - 1, core), at(x + 2, core)
        mright, mleft, mfar = at(x + 1, other), at(x + chips - 1, other), at(x + 2, other)
        self.out = {
            self.R0: (self.me, 0, self.right), self.R1: (self.me, 1, self.right),
            self.L1: (self.me, 1, self.left), self.L0: (self.me, 0, self.left),
            self.F0: (self.left, 0, self.right), self.F1: (self.right, 1, self.left),
            self.OWN: (self.me, None, self.mate),
            self.PL0: (self.left, 0, self.mate), self.PL1: (self.left, 1, self.mate),
            self.PR0: (self.right, 0, self.mate), self.PR1: (self.right, 1, self.mate),
            self.PO0: (self.far, 0, self.mate), self.PO1: (self.far, 1, self.mate),
        }
        self.inn = {
            self.R0: (self.left, 0), self.R1: (self.left, 1),
            self.L1: (self.right, 1), self.L0: (self.right, 0),
            self.F0: (self.far, 0), self.F1: (self.far, 1),
            self.OWN: (self.mate, None),
            self.PL0: (mleft, 0), self.PL1: (mleft, 1),
            self.PR0: (mright, 0), self.PR1: (mright, 1),
            self.PO0: (mfar, 0), self.PO1: (mfar, 1),
        }
        self.then = {
            self.R0: (self.F0, self.PL0), self.L1: (self.F1, self.PR1),
            self.R1: (self.PL1,), self.L0: (self.PR0,),
            self.F0: (self.PO0,), self.F1: (self.PO1,),
        }

    def ref(self, block, part):
        if part is None:
            return self.buf.at[block]
        return self.buf.at[block, pl.ds(part * self.half, self.half)]

    def copy(self, tag, block, part, to):
        ref = self.ref(block, part)
        return pltpu.make_async_remote_copy(
            ref, ref, self.send.at[tag], self.recv.at[tag], device_id={"tp": to}, device_id_type=MESH
        )

    def start(self):
        for tag in (self.R0, self.L1, self.R1, self.L0, self.OWN):
            self.copy(tag, *self.out[tag]).start()

    def arrive(self, *tags):
        for tag in tags:
            self.copy(tag, *self.inn[tag], self.mate).wait_recv()
            for later in self.then.get(tag, ()):
                self.copy(later, *self.out[later]).start()

    def finish(self):
        self.arrive(self.OWN, self.PL0, self.PR1, self.PL1, self.PR0, self.PO0, self.PO1)

    def drain(self):
        for tag in range(self.TAGS):
            self.copy(tag, *self.out[tag]).wait_send()


def kernel(
    zn, tn,
    tok_in, mix_gain, in_m, in_s, pool_m, pool_s, out_m, out_s, ffn_gain,
    gate_m, gate_s, up_m, up_s, gate_t, up_t, down_m, down_s,
    out_ref,
    tok, res, nf, io, inw, outg, outw, proj, pool, gu, par, lin, hid, dn, sbuf, rsb,
    load_sem, zsend, zrecv, gsend, grecv, osend, orecv, hsend, hrecv, dsend, drecv, rsend, rrecv,
):
    z, me = lax.axis_index("fs"), lax.axis_index("tp")
    x, core = lax.div(me, CORES), lax.rem(me, CORES)
    other = 1 - core
    mate = x * CORES + other
    chips = tn // CORES
    zright, zleft = lax.rem(z + 1, zn), lax.rem(z + zn - 1, zn)
    hops = zn // 2

    length, width = tok_in.shape
    depth, chan = in_m.shape
    ff = gate_m.shape[1]
    ocols = out_m.shape[1]
    full = ff // LANES
    tail = ff - full * LANES
    per = width // ocols

    load = pltpu.make_async_copy(tok_in, tok.at[me], load_sem)
    load.start()

    io[z, 0:depth, :] = in_m[...].astype(BF16)
    io[z, depth:, :] = (out_m[...] * out_s[...]).astype(BF16)

    def packed(g_ref, u_ref):
        for j in range(full):
            cols = slice(j * LANES, (j + 1) * LANES)
            yield 2 * j * LANES, jnp.concatenate([g_ref[:, cols], u_ref[:, cols]], axis=1)
        yield 2 * full * LANES, jnp.concatenate([g_ref[:, full * LANES :], u_ref[:, full * LANES :]], axis=1)

    own_rows = pl.ds(pl.multiple_of(z * depth, depth), depth)
    for at, v in packed(gate_m, up_m):
        gu[own_rows, at : at + v.shape[1]] = v.astype(BF16)
    for at, v in packed(gate_s, up_s):
        par[0:1, at : at + v.shape[1]] = v
    for at, v in packed(gate_t, up_t):
        par[1:4, at : at + v.shape[1]] = v
    dn[core, z, 0:ff, :] = (down_m[...] * down_s[...]).astype(BF16)
    dpad = dn.shape[2]

    def clear(i, _):
        dn[0, i, ff:dpad, :] = jnp.zeros((dpad - ff, ocols), BF16)
        dn[1, i, ff:dpad, :] = jnp.zeros((dpad - ff, ocols), BF16)
        return 0

    lax.fori_loop(0, zn, clear, 0)
    lin[0:8, :] = jnp.zeros((8, lin.shape[1]), F32)
    load.wait()

    barrier = pltpu.get_barrier_semaphore()
    for to in (zleft, zright):
        pl.semaphore_signal(barrier, inc=1, device_id={"fs": to}, device_id_type=MESH)
    for j in range(1, tn):
        pl.semaphore_signal(barrier, inc=1, device_id={"tp": lax.rem(me + j, tn)}, device_id_type=MESH)
    pl.semaphore_wait(barrier, tn + 1)

    def io_part(slot, part):
        n = 2 * depth
        if part is None:
            return io.at[slot]
        return io.at[slot, pl.ds(part * (n // 2), n // 2)]

    def gu_part(r0, n, first):
        def at(slot, part):
            a, m = ((r0, n), (r0, first), (r0 + first, n - first))[0 if part is None else part + 1]
            return gu.at[pl.ds(pl.multiple_of(slot * depth + a, 16), m)]

        return at

    def dn_part(r0, n):
        def at(slot, part):
            a, m = (r0, n) if part is None else (r0 + part * (n // 2), n // 2)
            return dn.at[core, slot, pl.ds(a, m)]

        return at

    q = depth // 8
    lanes = [
        io_part,
        gu_part(0, 2 * q, q),
        gu_part(2 * q, 3 * q, 2 * q),
        gu_part(5 * q, 3 * q, 2 * q),
        dn_part(0, ff // 2),
        dn_part(ff // 2, ff // 2),
    ]
    A, B0, B1, B2, C1, C2 = range(6)

    def zslot(d, s):
        return lax.rem(z + zn + (s if d else -s), zn)

    def zcopy(i, d, s, part, slot):
        ref = lanes[i](slot, part)
        return pltpu.make_async_remote_copy(
            ref, ref, zsend.at[i, d], zrecv.at[i, d, s - 1],
            device_id={"fs": zleft if d else zright}, device_id_type=MESH,
        )

    def zput(i, d, s, part=None):
        return zcopy(i, d, s, part, zslot(d, s - 1))

    def zgot(i, d, s, part=None):
        zcopy(i, d, s, part, zslot(d, s)).wait_recv()

    def zopen(i):
        for d in range(2):
            zput(i, d, 1).start()

    def tick(i, s):
        for d in range(2):
            static = isinstance(s, int)
            part = d if static and s == hops else None
            zgot(i, d, s, part)
            zput(i, d, s, part).wait_send()
            if not static or s < hops - 1:
                zput(i, d, s + 1).start()
            elif s == hops - 1:
                zput(i, d, s + 1, d).start()

    def steps():
        for s in range(1, hops + 1):
            tick(A, s)
            if s == hops - 1:
                zopen(B1)
            yield
            tick(B0, s)
            if s == hops - 1:
                zopen(B2)
            yield
        for s in range(1, hops + 1):
            tick(B1, s)
            if s == hops - 1:
                zopen(C1)
            yield
            tick(B2, s)
            if s == hops - 1:
                zopen(C2)
            yield

    ring = steps()

    def go(n):
        for _ in range(n):
            next(ring)

    gathers = [
        FeatureGather(buf, gsend.at[k], grecv.at[k], chips, x, core) for k, buf in enumerate((tok, pool, res))
    ]
    g_tok, g_pool, g_res = gathers
    G = FeatureGather

    def hand(d, s, which, slot):
        ref = dn.at[which, slot, pl.ds(0, ff)]
        return pltpu.make_async_remote_copy(
            ref, ref, dsend.at[d, s], drecv.at[d, s], device_id={"tp": mate}, device_id_type=MESH
        )

    zopen(A)
    zopen(B0)
    g_tok.start()
    hand(0, 0, core, z).start()

    def norm(buf, gain_ref, lo, hi):
        rows = 32

        def body(i, _):
            r = pl.ds(pl.multiple_of(i * rows, rows), rows)
            total = jnp.zeros((rows, width), F32)
            for p in range(tn):
                v = buf[p, r, :].astype(F32)
                total = total + v * v
            mean = jnp.sum(total, axis=1, keepdims=True) * (1.0 / (tn * width))
            scale = lax.rsqrt(mean + EPS)
            for p in range(tn):
                cols = slice(p * width, (p + 1) * width)
                nf[r, cols] = (buf[p, r, :].astype(F32) * scale * gain_ref[:, cols]).astype(BF16)
            return 0

        lax.fori_loop(lo // rows, hi // rows, body, 0)

    go(2)
    g_tok.arrive(G.R0, G.L1)
    go(4)
    g_tok.arrive(G.R1, G.L0)
    go(2)
    g_tok.arrive(G.F0, G.F1)
    go(2)
    g_tok.finish()
    norm(tok, mix_gain, 0, length // 2)
    go(2)
    norm(tok, mix_gain, length // 2, length)
    go(4)

    def own_rows_copy(j, block, to):
        return pltpu.make_async_remote_copy(
            io.at[pl.ds(to * per, per), pl.ds(depth, depth)], outg.at[block],
            osend.at[j], orecv.at[j], device_id={"tp": to}, device_id_type=MESH,
        )

    for j in range(1, tn):
        own_rows_copy(j, me, lax.rem(me + j, tn)).start()
    outg[me] = io[pl.ds(me * per, per), depth:, :]

    for k in range(zn):
        inw[k * depth : (k + 1) * depth, :] = io[k, 0:depth, :]
    tile = length // 4

    def project(i, _):
        r = pl.ds(pl.multiple_of(i * tile, tile), tile)
        v = jnp.dot(nf[r, :], inw[...], preferred_element_type=F32) * in_s[...]
        proj[r, :] = v.astype(BF16).astype(F32)
        return 0

    lax.fori_loop(0, 4, project, 0)

    v = proj[...]
    row = lax.broadcasted_iota(jnp.int32, v.shape, 0)

    def back(a, k):
        return jnp.where(row >= k, pltpu.roll(a, k, 0), 0.0)

    s2 = v + back(v, 1)
    s4 = s2 + back(s2, 2)
    s8 = s4 + back(s4, 4)
    s16 = s8 + back(s8, 8)
    total = jnp.where(x == 0, s2, jnp.where(x == 1, s4, jnp.where(x == 2, s8, s16)))
    count = jnp.minimum(row + 1, lax.shift_left(jnp.int32(2), x)).astype(F32)
    spread = (total / count - v).astype(BF16)
    mixed = jnp.dot(spread, pool_m[0], preferred_element_type=F32) * pool_s[...]
    pool[me] = mixed.astype(BF16)
    g_pool.start()

    go(2)
    g_pool.arrive(G.R0, G.L1)
    for j in range(1, tn):
        own_rows_copy(j, lax.rem(me + tn - j, tn), mate).wait_recv()
    for p in range(tn):
        for k in range(per):
            outw[p * chan : (p + 1) * chan, k * ocols : (k + 1) * ocols] = outg[p, k]
    g_pool.arrive(G.R1, G.L0)
    go(2)
    g_pool.arrive(G.F0, G.F1)
    g_pool.finish()

    def mix(i, _):
        r = pl.ds(pl.multiple_of(i * tile, tile), tile)
        rows = jnp.concatenate([pool[p, r, :] for p in range(tn)], axis=1)
        v = jnp.dot(rows, outw[...], preferred_element_type=F32)
        res[me, r, :] = (tok[me, r, :].astype(F32) + v).astype(BF16)
        return 0

    lax.fori_loop(0, 4, mix, 0)
    g_res.start()
    go(3)
    g_res.arrive(G.R0, G.L1)
    go(2)
    g_res.arrive(G.R1, G.L0)
    go(3)
    g_res.arrive(G.F0, G.F1)
    g_res.finish()
    go(1)
    norm(res, ffn_gain, 0, length // 2)
    go(2)
    norm(res, ffn_gain, length // 2, length)
    go(1)

    taps = lin.shape[0] - length

    def tile_product(at, n):
        def body(i, _):
            r = pl.ds(pl.multiple_of(i * tile, tile), tile)
            v = jnp.dot(nf[r, :], gu[:, pl.ds(at, n)], preferred_element_type=F32)
            v = (v * par[0:1, pl.ds(at, n)]).astype(BF16).astype(F32)
            lin[pl.ds(pl.multiple_of(taps + i * tile, 8), tile), 0:n] = v
            return 0

        lax.fori_loop(0, 4, body, 0)

    chunk = 64

    def convolved(i, at, off):
        w = lin[pl.ds(pl.multiple_of(i * chunk, 8), chunk + taps), off : off + LANES]
        t = par[:, pl.ds(at + off, LANES)]
        return (
            t[3:4] * w[taps:] + t[2:3] * pltpu.roll(w, 1, 0)[taps:] + t[1:2] * pltpu.roll(w, 2, 0)[taps:]
        )

    def silu(g):
        return g / (1.0 + jnp.exp(-g))

    def hcopy(j, which):
        ref = hid.at[which, j]
        return pltpu.make_async_remote_copy(
            ref, ref, hsend.at[j], hrecv.at[j], device_id={"tp": mate}, device_id_type=MESH
        )

    def column(j):
        at = pl.multiple_of(j * 2 * LANES, 2 * LANES)
        tile_product(at, 2 * LANES)

        def body(i, _):
            r = pl.ds(pl.multiple_of(i * chunk, chunk), chunk)
            h = silu(convolved(i, at, 0)) * convolved(i, at, LANES)
            hid[core, j, r, :] = h.astype(BF16)
            return 0

        lax.fori_loop(0, length // chunk, body, 0)
        hcopy(j, core).start()

    def two_columns(k, _):
        column(2 * k)
        tick(C1, k + 1)
        column(2 * k + 1)
        tick(C2, k + 1)
        return 0

    lax.fori_loop(0, full // 2, two_columns, 0)
    for j in range(full // 2 * 2, full):
        column(j)
    ahead = full // 2 + 1
    tick(C1, ahead)
    last = 2 * full * LANES
    tile_product(last, LANES)
    lane = lax.broadcasted_iota(jnp.int32, (chunk, LANES), 1)

    def narrow(i, _):
        r = pl.ds(pl.multiple_of(i * chunk, chunk), chunk)
        y = convolved(i, last, 0)
        h = jnp.where(lane < tail, silu(y) * pltpu.roll(y, LANES - tail, 1), 0.0)
        hid[core, full, r, :] = h.astype(BF16)
        return 0

    lax.fori_loop(0, length // chunk, narrow, 0)
    hcopy(full, core).start()
    tick(C2, ahead)

    def toward(m, p, src_chip):
        return pltpu.make_async_remote_copy(
            sbuf.at[m, p], rsb.at[src_chip, p], rsend.at[m, p], rrecv.at[src_chip, p],
            device_id={"tp": m * CORES + core}, device_id_type=MESH,
        )

    def block(slot):
        owner = lax.div(slot, per)
        m, p = lax.div(owner, CORES), lax.rem(slot, per)

        @pl.when(lax.rem(owner, CORES) == core)
        def _():
            def body(i, _):
                r = pl.ds(pl.multiple_of(i * tile, tile), tile)
                rows = jnp.concatenate([hid[k, j, r, :] for k in range(CORES) for j in range(full + 1)], axis=1)
                cols = jnp.concatenate([dn[k, slot] for k in range(CORES)], axis=0)
                sbuf[m, p, r, :] = jnp.dot(rows, cols, preferred_element_type=F32).astype(BF16)
                return 0

            lax.fori_loop(0, 4, body, 0)

            @pl.when(m != x)
            def _():
                toward(m, p, x).start()

    def pass_over(s):
        for d in range(2):
            hand(d, s, core, zslot(d, s)).start()

    def both(s):
        for d in range(2):
            slot = zslot(d, s)
            hand(d, s, other, slot).wait_recv()
            block(slot)

    lax.fori_loop(1, ahead + 1, lambda s, _: (pass_over(s), 0)[1], 0)
    for j in range(full + 1):
        hcopy(j, other).wait_recv()
    hand(0, 0, other, z).wait_recv()
    block(z)
    lax.fori_loop(1, ahead, lambda s, _: (both(s), 0)[1], 0)

    def onward(s, _):
        tick(C1, s)
        tick(C2, s)
        pass_over(s)
        both(s - 1)
        return 0

    lax.fori_loop(ahead + 1, hops - 1, onward, 0)
    onward(hops - 1, 0)
    both(hops - 1)
    tick(C1, hops)
    tick(C2, hops)
    end = zslot(0, hops)
    hand(0, hops, core, end).start()
    hand(0, hops, other, end).wait_recv()
    block(end)

    for j in range(1, chips):
        src = lax.rem(x + j, chips)
        for p in range(per):
            toward(x, p, src).wait_recv()

    def total_rows(i, _):
        r = pl.ds(pl.multiple_of(i * tile, tile), tile)
        for p in range(per):
            cols = slice(p * ocols, (p + 1) * ocols)
            v = res[me, r, cols].astype(F32) + sbuf[x, p, r, :].astype(F32)
            for j in range(1, chips):
                v = v + rsb[lax.rem(x + j, chips), p, r, :].astype(F32)
            out_ref[r, cols] = v.astype(BF16)
        return 0

    lax.fori_loop(0, 4, total_rows, 0)

    for g in gathers:
        g.drain()
    for j in range(1, tn):
        own_rows_copy(j, me, lax.rem(me + j, tn)).wait_send()
    for j in range(full + 1):
        hcopy(j, core).wait_send()
    hand(0, 0, core, z).wait_send()
    for s in range(1, hops):
        for d in range(2):
            hand(d, s, core, zslot(d, s)).wait_send()
    hand(0, hops, core, end).wait_send()
    for j in range(1, chips):
        for p in range(per):
            toward(lax.rem(x + j, chips), p, x).wait_send()


def layer(zn, tn, tokens, mix_gain, in_m, in_s, pool_m, pool_s, out_m, out_s, ffn_gain,
          gate_m, gate_s, up_m, up_s, gate_t, up_t, down_m, down_s):
    _, length, width = tokens.shape
    depth, chan = in_m.shape
    ff = gate_m.shape[1]
    ocols = out_m.shape[1]
    per = width // ocols
    assert ff % LANES == LANES // 2 and per == 2 and chan == LANES
    tiles = ff // LANES + 1
    chips = tn // CORES
    hops = zn // 2
    dma = pltpu.SemaphoreType.DMA
    vmem = pl.BlockSpec(memory_space=pltpu.VMEM)
    out = pl.pallas_call(
        functools.partial(kernel, zn, tn),
        out_shape=jax.ShapeDtypeStruct((length, width), BF16),
        in_specs=[pl.BlockSpec(memory_space=pl.ANY)] + [vmem] * 16,
        out_specs=vmem,
        scratch_shapes=[
            pltpu.VMEM((tn, length, width), BF16),
            pltpu.VMEM((tn, length, width), BF16),
            pltpu.VMEM((length, tn * width), BF16),
            pltpu.VMEM((zn, 2 * depth, chan), BF16),
            pltpu.VMEM((zn * depth, chan), BF16),
            pltpu.VMEM((tn, per, chan, ocols), BF16),
            pltpu.VMEM((tn * chan, width), BF16),
            pltpu.VMEM((length, chan), F32),
            pltpu.VMEM((tn, length, chan), BF16),
            pltpu.VMEM((zn * depth, 2 * ff), BF16),
            pltpu.VMEM((8, 2 * ff), F32),
            pltpu.VMEM((length + 8, 2 * LANES), F32),
            pltpu.VMEM((CORES, tiles, length, LANES), BF16),
            pltpu.VMEM((CORES, zn, tiles * LANES, ocols), BF16),
            pltpu.VMEM((chips, per, length, ocols), BF16),
            pltpu.VMEM((chips, per, length, ocols), BF16),
            dma,
            dma((6, 2)), dma((6, 2, hops)),
            dma((3, FeatureGather.TAGS)), dma((3, FeatureGather.TAGS)),
            dma((tn,)), dma((tn,)),
            dma((tiles,)), dma((tiles,)),
            dma((2, hops + 1)), dma((2, hops + 1)),
            dma((chips, per)), dma((chips, per)),
        ],
        compiler_params=pltpu.CompilerParams(
            collective_id=0, has_side_effects=True, vmem_limit_bytes=66_000_000
        ),
    )(
        tokens.reshape(length, width), mix_gain.reshape(1, -1), in_m, in_s, pool_m, pool_s, out_m, out_s,
        ffn_gain.reshape(1, -1), gate_m, gate_s, up_m, up_s, gate_t, up_t, down_m, down_s,
    )
    return out.reshape(tokens.shape)


def solution(mesh):
    return jax.shard_map(
        functools.partial(layer, mesh.shape["fs"], mesh.shape["tp"]),
        mesh=mesh,
        in_specs=(
            P(("grp", "fs"), None, "tp"),
            P(),
            P("fs", "tp"),
            P(None, "tp"),
            P("tp", None, None),
            P(None, "tp"),
            P("tp", "fs"),
            P(None, "fs"),
            P(),
            P("fs", "tp"),
            P(None, "tp"),
            P("fs", "tp"),
            P(None, "tp"),
            P(None, "tp"),
            P(None, "tp"),
            P("tp", "fs"),
            P(None, "fs"),
        ),
        out_specs=P(("grp", "fs"), None, "tp"),
        check_vma=False,
    )
```

time: 364 us -> 178 us (0.49)
  the two profiles are of different devices: /device:TPU:33 before, /device:TPU:292 now
where the time goes in v1:
time: 178 us; the launch traced here: 177 us
  Pallas kernels  173 us (97%)
  local copies, waits for them, and re-layouts  4.74 us (3%)
    pallas_call x1, Pallas kernels, layer(): pl.pallas_call(functools.partial(kernel, zn, tn), out_shape=jax.ShapeDtyp...  173 us
    unnamed x5, local copies, waits for them, and re-layouts  4.74 us

profile of v1, /device:TPU:292, one launch (start us, length us, event | category | flops | bytes accessed | tf_op | source)
XLA Modules:
  0.0 177.5 jit_solution(4278632229284159945)
XLA Ops:
  0.0 0.0 copy-start
  0.0 1.9 %copy.18.gate_m = f32[128,704]{1,0:T(8,128)} copy(f32[128,704]{0,1:T(8,128)} %param.26) | data formatting | bytes 720896 | tf_op args[9]
  1.9 0.0 copy-done
  2.0 0.9 copy.19.up_m
  2.9 172.7 %shard_map.163 = bf16[1024,256]{1,0:T(8,128)(2,1)} custom-call(bf16[1024,256]{1,0:T(8,128)(2,1)} %bitcast.5, f32[1,2048]{1,0:T(1,128)} %bitcast.6, f32[128,128]{1,0:T(8,128)} %in_m.1, f32[1,128]{1,0:T(1,128)} %in_s.1, bf16[1,128,128]{2,1,0:T(8,128)(2,1)} %pool_m.1, f32[1,128]{1,0:T(1,128)} %pool_s.1, f32[128,128]{1,0:T(8,128)} %out_m.1, f32[1,128]{1,0:T(1,128)} %out_s.1, ...), custom_call_target="tpu_custom_call" | custom-call | tf_op jit(solution)/shard_map/pallas_call | solution.py:529
  175.6 1.9 %copy.21 = bf16[1,1024,256]{2,1,0:T(8,128)(2,1)} copy(bf16[1,1024,256]{2,1,0:T(8,128)(2,1)} %bitcast.4) | data formatting | bytes 1048576
Async XLA Ops:
  0.0 2.0 %copy-start = (f32[128,704]{0,1:T(8,128)S(1)}, f32[128,704]{0,1:T(8,128)}, u32[]{:S(2)}) copy-start(f32[128,704]{0,1:T(8,128)} %param.28) | copy-start | bytes 1081348

commit v2 on v1

--- a/solution.py
+++ b/solution.py
@@ -85,10 +85,13 @@
     tok_in, mix_gain, in_m, in_s, pool_m, pool_s, out_m, out_s, ffn_gain,
     gate_m, gate_s, up_m, up_s, gate_t, up_t, down_m, down_s,
     out_ref,
-    tok, res, nf, io, inw, outg, outw, proj, pool, gu, par, lin, hid, dn, sbuf, rsb,
-    load_sem, zsend, zrecv, gsend, grecv, osend, orecv, hsend, hrecv, dsend, drecv, rsend, rrecv,
+    tok, res, nf, io, inw, outg, outw, proj, pool, gu, par, lin, hid, dn, sums, far, near,
+    load_sem, zsend, zrecv, gsend, grecv, osend, orecv, hsend, hrecv, dsend, drecv,
+    ysend, yrecv, fsend, frecv, rsend, rrecv,
 ):
-    z, me = lax.axis_index("fs"), lax.axis_index("tp")
+    z, me, group = lax.axis_index("fs"), lax.axis_index("tp"), lax.axis_index("grp")
+    side = lax.rem(group, 2)
+    twin = group + 1 - 2 * side
     x, core = lax.div(me, CORES), lax.rem(me, CORES)
     other = 1 - core
     mate = x * CORES + other
@@ -98,7 +101,7 @@
 
     length, width = tok_in.shape
     depth, chan = in_m.shape
-    ff = gate_m.shape[1]
+    ff = gate_m.shape[0]
     ocols = out_m.shape[1]
     full = ff // LANES
     tail = ff - full * LANES
@@ -117,8 +120,12 @@
         yield 2 * full * LANES, jnp.concatenate([g_ref[:, full * LANES :], u_ref[:, full * LANES :]], axis=1)
 
     own_rows = pl.ds(pl.multiple_of(z * depth, depth), depth)
-    for at, v in packed(gate_m, up_m):
-        gu[own_rows, at : at + v.shape[1]] = v.astype(BF16)
+    for j in range(full):
+        for k, ref in enumerate((gate_m, up_m)):
+            at = (2 * j + k) * LANES
+            gu[own_rows, at : at + LANES] = ref[j * LANES : (j + 1) * LANES, :].T.astype(BF16)
+    rest = jnp.concatenate([gate_m[full * LANES :, :], up_m[full * LANES :, :]], axis=0)
+    gu[own_rows, 2 * full * LANES :] = rest.T.astype(BF16)
     for at, v in packed(gate_s, up_s):
         par[0:1, at : at + v.shape[1]] = v
     for at, v in packed(gate_t, up_t):
@@ -140,7 +147,8 @@
         pl.semaphore_signal(barrier, inc=1, device_id={"fs": to}, device_id_type=MESH)
     for j in range(1, tn):
         pl.semaphore_signal(barrier, inc=1, device_id={"tp": lax.rem(me + j, tn)}, device_id_type=MESH)
-    pl.semaphore_wait(barrier, tn + 1)
+    pl.semaphore_signal(barrier, inc=1, device_id={"grp": twin}, device_id_type=MESH)
+    pl.semaphore_wait(barrier, tn + 2)
 
     def io_part(slot, part):
         n = 2 * depth
@@ -148,12 +156,15 @@
             return io.at[slot]
         return io.at[slot, pl.ds(part * (n // 2), n // 2)]
 
-    def gu_part(r0, n, first):
-        def at(slot, part):
-            a, m = ((r0, n), (r0, first), (r0 + first, n - first))[0 if part is None else part + 1]
-            return gu.at[pl.ds(pl.multiple_of(slot * depth + a, 16), m)]
-
-        return at
+    half = depth // 2
+    cut = half // 2
+
+    def gu_rows(b, slot, whose, part):
+        a, m = (b * cut, cut) if part is None else (b * cut + part * (cut // 2), cut // 2)
+        return gu.at[pl.ds(pl.multiple_of(slot * depth + whose * half + a, 16), m)]
+
+    def gu_part(b):
+        return lambda slot, part: gu_rows(b, slot, side, part)
 
     def dn_part(r0, n):
         def at(slot, part):
@@ -162,16 +173,8 @@
 
         return at
 
-    q = depth // 8
-    lanes = [
-        io_part,
-        gu_part(0, 2 * q, q),
-        gu_part(2 * q, 3 * q, 2 * q),
-        gu_part(5 * q, 3 * q, 2 * q),
-        dn_part(0, ff // 2),
-        dn_part(ff // 2, ff // 2),
-    ]
-    A, B0, B1, B2, C1, C2 = range(6)
+    lanes = [io_part, gu_part(0), gu_part(1), dn_part(0, ff // 2), dn_part(ff // 2, ff // 2)]
+    A, B1, B2, C1, C2 = range(5)
 
     def zslot(d, s):
         return lax.rem(z + zn + (s if d else -s), zn)
@@ -203,25 +206,71 @@
                 zput(i, d, s + 1).start()
             elif s == hops - 1:
                 zput(i, d, s + 1, d).start()
+            if not static or s < hops:
+                handed(i, d, s)
+        if isinstance(s, int) and s == hops:
+            handed(i, 0, s)
+
+    def ycopy(b, d, s, whose):
+        ref = gu_rows(b, zslot(d, s), whose, None)
+        return pltpu.make_async_remote_copy(
+            ref, ref, ysend.at[b, d, s], yrecv.at[b, d, s], device_id={"grp": twin}, device_id_type=MESH
+        )
+
+    def hand(c, d, s, which):
+        ref = dn.at[which, zslot(d, s), pl.ds(c * (ff // 2), ff // 2)]
+        return pltpu.make_async_remote_copy(
+            ref, ref, dsend.at[c, d, s], drecv.at[c, d, s], device_id={"tp": mate}, device_id_type=MESH
+        )
+
+    def ocopy(slot, src):
+        owner = lax.div(slot, per)
+        return pltpu.make_async_remote_copy(
+            io.at[slot, pl.ds(depth, depth)], outg.at[src, lax.rem(slot, per)],
+            osend.at[slot], orecv.at[src, lax.rem(slot, per)],
+            device_id={"tp": owner}, device_id_type=MESH,
+        )
+
+    def handed(i, d, s):
+        if i == A:
+            slot = zslot(d, s)
+
+            @pl.when(lax.div(slot, per) != me)
+            def _():
+                ocopy(slot, me).start()
+        elif i in (B1, B2):
+            ycopy(i - B1, d, s, side).start()
+        else:
+            hand(i - C1, d, s, core).start()
+
+
+    def each_arrival(fn):
+        fn(0, 0)
+
+        def body(s, _):
+            fn(0, s)
+            fn(1, s)
+            return 0
+
+        lax.fori_loop(1, hops, body, 0)
+        fn(0, hops)
 
     def steps():
         for s in range(1, hops + 1):
             tick(A, s)
             if s == hops - 1:
-                zopen(B1)
-            yield
-            tick(B0, s)
-            if s == hops - 1:
                 zopen(B2)
-            yield
-        for s in range(1, hops + 1):
             tick(B1, s)
             if s == hops - 1:
                 zopen(C1)
             yield
+        for s in range(1, hops + 1):
             tick(B2, s)
-            if s == hops - 1:
+            tick(C1, s)
+            if s == hops - 2:
                 zopen(C2)
+            if s > hops - 2:
+                tick(C2, s + 2 - hops)
             yield
 
     ring = steps()
@@ -236,16 +285,11 @@
     g_tok, g_pool, g_res = gathers
     G = FeatureGather
 
-    def hand(d, s, which, slot):
-        ref = dn.at[which, slot, pl.ds(0, ff)]
-        return pltpu.make_async_remote_copy(
-            ref, ref, dsend.at[d, s], drecv.at[d, s], device_id={"tp": mate}, device_id_type=MESH
-        )
-
     zopen(A)
-    zopen(B0)
+    zopen(B1)
     g_tok.start()
-    hand(0, 0, core, z).start()
+    for i in (A, B1, B2, C1, C2):
+        handed(i, 0, 0)
 
     def norm(buf, gain_ref, lo, hi):
         rows = 32
@@ -267,26 +311,19 @@
 
     go(2)
     g_tok.arrive(G.R0, G.L1)
-    go(4)
+    go(1)
     g_tok.arrive(G.R1, G.L0)
     go(2)
     g_tok.arrive(G.F0, G.F1)
-    go(2)
     g_tok.finish()
-    norm(tok, mix_gain, 0, length // 2)
-    go(2)
-    norm(tok, mix_gain, length // 2, length)
-    go(4)
-
-    def own_rows_copy(j, block, to):
-        return pltpu.make_async_remote_copy(
-            io.at[pl.ds(to * per, per), pl.ds(depth, depth)], outg.at[block],
-            osend.at[j], orecv.at[j], device_id={"tp": to}, device_id_type=MESH,
-        )
-
-    for j in range(1, tn):
-        own_rows_copy(j, me, lax.rem(me + j, tn)).start()
-    outg[me] = io[pl.ds(me * per, per), depth:, :]
+    part = length // 4
+    norm(tok, mix_gain, 0, part)
+    go(1)
+    norm(tok, mix_gain, part, 2 * part)
+    norm(tok, mix_gain, 2 * part, 3 * part)
+    go(1)
+    norm(tok, mix_gain, 3 * part, length)
+    go(1)
 
     for k in range(zn):
         inw[k * depth : (k + 1) * depth, :] = io[k, 0:depth, :]
@@ -317,16 +354,24 @@
     pool[me] = mixed.astype(BF16)
     g_pool.start()
 
-    go(2)
+    go(1)
     g_pool.arrive(G.R0, G.L1)
-    for j in range(1, tn):
-        own_rows_copy(j, lax.rem(me + tn - j, tn), mate).wait_recv()
+
+    def others(fn):
+        for j in range(1, tn):
+            for k in range(per):
+                fn(lax.rem(me + j, tn), k)
+
+    others(lambda p, k: ocopy(me * per + k, p).wait_recv())
+    for k in range(per):
+        outg[me, k] = io[me * per + k, depth:, :]
     for p in range(tn):
         for k in range(per):
             outw[p * chan : (p + 1) * chan, k * ocols : (k + 1) * ocols] = outg[p, k]
+    go(1)
     g_pool.arrive(G.R1, G.L0)
-    go(2)
     g_pool.arrive(G.F0, G.F1)
+    go(1)
     g_pool.finish()
 
     def mix(i, _):
@@ -338,18 +383,18 @@
 
     lax.fori_loop(0, 4, mix, 0)
     g_res.start()
-    go(3)
+    go(2)
     g_res.arrive(G.R0, G.L1)
-    go(2)
+    go(1)
     g_res.arrive(G.R1, G.L0)
-    go(3)
+    go(1)
     g_res.arrive(G.F0, G.F1)
     g_res.finish()
-    go(1)
     norm(res, ffn_gain, 0, length // 2)
-    go(2)
+    go(1)
     norm(res, ffn_gain, length // 2, length)
-    go(1)
+    for b in range(2):
+        each_arrival(lambda d, s, b=b: ycopy(b, d, s, 1 - side).wait_recv())
 
     taps = lin.shape[0] - length
 
@@ -394,18 +439,16 @@
         lax.fori_loop(0, length // chunk, body, 0)
         hcopy(j, core).start()
 
-    def two_columns(k, _):
-        column(2 * k)
-        tick(C1, k + 1)
-        column(2 * k + 1)
-        tick(C2, k + 1)
+    early = 3
+
+    def some_columns(j, _):
+        column(j)
+        tick(C2, j + early)
         return 0
 
-    lax.fori_loop(0, full // 2, two_columns, 0)
-    for j in range(full // 2 * 2, full):
-        column(j)
-    ahead = full // 2 + 1
-    tick(C1, ahead)
+    lax.fori_loop(0, full - 1, some_columns, 0)
+    column(full - 1)
+    tick(C2, full - 1 + early)
     last = 2 * full * LANES
     tile_product(last, LANES)
     lane = lax.broadcasted_iota(jnp.int32, (chunk, LANES), 1)
@@ -419,110 +462,116 @@
 
     lax.fori_loop(0, length // chunk, narrow, 0)
     hcopy(full, core).start()
-    tick(C2, ahead)
-
-    def toward(m, p, src_chip):
-        return pltpu.make_async_remote_copy(
-            sbuf.at[m, p], rsb.at[src_chip, p], rsend.at[m, p], rrecv.at[src_chip, p],
-            device_id={"tp": m * CORES + core}, device_id_type=MESH,
-        )
-
-    def block(slot):
-        owner = lax.div(slot, per)
-        m, p = lax.div(owner, CORES), lax.rem(slot, per)
-
-        @pl.when(lax.rem(owner, CORES) == core)
-        def _():
-            def body(i, _):
-                r = pl.ds(pl.multiple_of(i * tile, tile), tile)
-                rows = jnp.concatenate([hid[k, j, r, :] for k in range(CORES) for j in range(full + 1)], axis=1)
-                cols = jnp.concatenate([dn[k, slot] for k in range(CORES)], axis=0)
-                sbuf[m, p, r, :] = jnp.dot(rows, cols, preferred_element_type=F32).astype(BF16)
-                return 0
-
-            lax.fori_loop(0, 4, body, 0)
-
-            @pl.when(m != x)
-            def _():
-                toward(m, p, x).start()
-
-    def pass_over(s):
-        for d in range(2):
-            hand(d, s, core, zslot(d, s)).start()
-
-    def both(s):
-        for d in range(2):
-            slot = zslot(d, s)
-            hand(d, s, other, slot).wait_recv()
-            block(slot)
-
-    lax.fori_loop(1, ahead + 1, lambda s, _: (pass_over(s), 0)[1], 0)
+    tick(C2, hops)
+
     for j in range(full + 1):
         hcopy(j, other).wait_recv()
-    hand(0, 0, other, z).wait_recv()
-    block(z)
-    lax.fori_loop(1, ahead, lambda s, _: (both(s), 0)[1], 0)
-
-    def onward(s, _):
-        tick(C1, s)
-        tick(C2, s)
-        pass_over(s)
-        both(s - 1)
-        return 0
-
-    lax.fori_loop(ahead + 1, hops - 1, onward, 0)
-    onward(hops - 1, 0)
-    both(hops - 1)
-    tick(C1, hops)
-    tick(C2, hops)
-    end = zslot(0, hops)
-    hand(0, hops, core, end).start()
-    hand(0, hops, other, end).wait_recv()
-    block(end)
-
-    for j in range(1, chips):
-        src = lax.rem(x + j, chips)
-        for p in range(per):
-            toward(x, p, src).wait_recv()
-
-    def total_rows(i, _):
-        r = pl.ds(pl.multiple_of(i * tile, tile), tile)
-        for p in range(per):
-            cols = slice(p * ocols, (p + 1) * ocols)
-            v = res[me, r, cols].astype(F32) + sbuf[x, p, r, :].astype(F32)
-            for j in range(1, chips):
-                v = v + rsb[lax.rem(x + j, chips), p, r, :].astype(F32)
-            out_ref[r, cols] = v.astype(BF16)
-        return 0
-
-    lax.fori_loop(0, 4, total_rows, 0)
+    for c in range(2):
+        each_arrival(lambda d, s, c=c: hand(c, d, s, other).wait_recv())
+
+    at_chip = lambda m: lax.rem(m, chips) * CORES + core
+    FAR, RIGHT, LEFT, OWN = range(4)
+    owner_of = (x + 2, x + 1, x + chips - 1, x)
+    side_rows = length // 2
+
+    def down(which, h, extra=None):
+        m = lax.rem(owner_of[which], chips)
+        slot = (m * CORES + core) * per
+
+        def body(i, _):
+            r = pl.ds(pl.multiple_of(h * side_rows + i * tile, tile), tile)
+            rows = jnp.concatenate([hid[k, j, r, :] for k in range(CORES) for j in range(full + 1)], axis=1)
+            cols = jnp.concatenate(
+                [jnp.concatenate([dn[k, slot + p] for p in range(per)], axis=1) for k in range(CORES)], axis=0
+            )
+            v = jnp.dot(rows, cols, preferred_element_type=F32)
+            if extra is not None:
+                v = v + far[extra, pl.ds(pl.multiple_of(i * tile, tile), tile), :].astype(F32)
+            sums[which, r, :] = v.astype(BF16)
+            return 0
+
+        lax.fori_loop(0, side_rows // tile, body, 0)
+
+    def half_rows(h):
+        return pl.ds(h * side_rows, side_rows)
+
+    def far_copy(h):
+        return pltpu.make_async_remote_copy(
+            sums.at[FAR, half_rows(h)], far.at[h], fsend.at[h], frecv.at[h],
+            device_id={"tp": at_chip(x + chips - 1 if h else x + 1)}, device_id_type=MESH,
+        )
+
+    def near_copy(which, h):
+        k = which - RIGHT
+        return pltpu.make_async_remote_copy(
+            sums.at[which, half_rows(h)], near.at[k, half_rows(h)], rsend.at[k, h], rrecv.at[k, h],
+            device_id={"tp": at_chip(owner_of[which])}, device_id_type=MESH,
+        )
+
+    down(FAR, 0)
+    far_copy(0).start()
+    down(FAR, 1)
+    far_copy(1).start()
+    down(RIGHT, 1)
+    near_copy(RIGHT, 1).start()
+    down(LEFT, 0)
+    near_copy(LEFT, 0).start()
+    down(OWN, 0)
+    far_copy(0).wait_recv()
+    down(RIGHT, 0, 0)
+    near_copy(RIGHT, 0).start()
+    far_copy(1).wait_recv()
+    down(LEFT, 1, 1)
+    near_copy(LEFT, 1).start()
+    down(OWN, 1)
+
+    def total_rows(h):
+        def body(i, _):
+            r = pl.ds(pl.multiple_of(h * side_rows + i * tile, tile), tile)
+            v = res[me, r, :].astype(F32) + sums[OWN, r, :].astype(F32)
+            for k in range(2):
+                v = v + near[k, r, :].astype(F32)
+            out_ref[r, :] = v.astype(BF16)
+            return 0
+
+        lax.fori_loop(0, side_rows // tile, body, 0)
+
+    for which, h in ((RIGHT, 1), (LEFT, 0), (RIGHT, 0), (LEFT, 1)):
+        near_copy(which, h).wait_recv()
+    for h in range(2):
+        total_rows(h)
 
     for g in gathers:
         g.drain()
-    for j in range(1, tn):
-        own_rows_copy(j, me, lax.rem(me + j, tn)).wait_send()
     for j in range(full + 1):
         hcopy(j, core).wait_send()
-    hand(0, 0, core, z).wait_send()
-    for s in range(1, hops):
-        for d in range(2):
-            hand(d, s, core, zslot(d, s)).wait_send()
-    hand(0, hops, core, end).wait_send()
-    for j in range(1, chips):
-        for p in range(per):
-            toward(lax.rem(x + j, chips), p, x).wait_send()
-
-
-def layer(zn, tn, tokens, mix_gain, in_m, in_s, pool_m, pool_s, out_m, out_s, ffn_gain,
+
+    def outs_left(slot, _):
+        @pl.when(lax.div(slot, per) != me)
+        def _():
+            ocopy(slot, me).wait_send()
+
+        return 0
+
+    lax.fori_loop(0, zn, outs_left, 0)
+    for b in range(2):
+        each_arrival(lambda d, s, b=b: ycopy(b, d, s, side).wait_send())
+        each_arrival(lambda d, s, b=b: hand(b, d, s, core).wait_send())
+    for h in range(2):
+        far_copy(h).wait_send()
+        near_copy(RIGHT, h).wait_send()
+        near_copy(LEFT, h).wait_send()
+
+
+def layer(gn, zn, tn, tokens, mix_gain, in_m, in_s, pool_m, pool_s, out_m, out_s, ffn_gain,
           gate_m, gate_s, up_m, up_s, gate_t, up_t, down_m, down_s):
     _, length, width = tokens.shape
     depth, chan = in_m.shape
     ff = gate_m.shape[1]
     ocols = out_m.shape[1]
     per = width // ocols
-    assert ff % LANES == LANES // 2 and per == 2 and chan == LANES
+    assert ff % LANES == LANES // 2 and per == 2 and chan == LANES and tn == 4 * CORES and gn % 2 == 0
     tiles = ff // LANES + 1
-    chips = tn // CORES
     hops = zn // 2
     dma = pltpu.SemaphoreType.DMA
     vmem = pl.BlockSpec(memory_space=pltpu.VMEM)
@@ -546,29 +595,32 @@
             pltpu.VMEM((length + 8, 2 * LANES), F32),
             pltpu.VMEM((CORES, tiles, length, LANES), BF16),
             pltpu.VMEM((CORES, zn, tiles * LANES, ocols), BF16),
-            pltpu.VMEM((chips, per, length, ocols), BF16),
-            pltpu.VMEM((chips, per, length, ocols), BF16),
+            pltpu.VMEM((4, length, width), BF16),
+            pltpu.VMEM((2, length // 2, width), BF16),
+            pltpu.VMEM((2, length, width), BF16),
             dma,
-            dma((6, 2)), dma((6, 2, hops)),
+            dma((5, 2)), dma((5, 2, hops)),
             dma((3, FeatureGather.TAGS)), dma((3, FeatureGather.TAGS)),
-            dma((tn,)), dma((tn,)),
+            dma((zn,)), dma((tn, per)),
             dma((tiles,)), dma((tiles,)),
-            dma((2, hops + 1)), dma((2, hops + 1)),
-            dma((chips, per)), dma((chips, per)),
+            dma((2, 2, hops + 1)), dma((2, 2, hops + 1)),
+            dma((2, 2, hops + 1)), dma((2, 2, hops + 1)),
+            dma((2,)), dma((2,)),
+            dma((2, 2)), dma((2, 2)),
         ],
         compiler_params=pltpu.CompilerParams(
             collective_id=0, has_side_effects=True, vmem_limit_bytes=66_000_000
         ),
     )(
         tokens.reshape(length, width), mix_gain.reshape(1, -1), in_m, in_s, pool_m, pool_s, out_m, out_s,
-        ffn_gain.reshape(1, -1), gate_m, gate_s, up_m, up_s, gate_t, up_t, down_m, down_s,
+        ffn_gain.reshape(1, -1), gate_m.T, gate_s, up_m.T, up_s, gate_t, up_t, down_m, down_s,
     )
     return out.reshape(tokens.shape)
 
 
 def solution(mesh):
     return jax.shard_map(
-        functools.partial(layer, mesh.shape["fs"], mesh.shape["tp"]),
+        functools.partial(layer, mesh.shape["grp"], mesh.shape["fs"], mesh.shape["tp"]),
         mesh=mesh,
         in_specs=(
             P(("grp", "fs"), None, "tp"),

time: 178 us -> 155 us (0.87)
  the two profiles are of different devices: /device:TPU:292 before, /device:TPU:33 now
where the time goes in v2:
time: 155 us
  Pallas kernels  153 us (99%)
  local copies, waits for them, and re-layouts  1.87 us (1%)
    pallas_call x1, Pallas kernels, layer(): pl.pallas_call(functools.partial(kernel, zn, tn), out_shape=jax.ShapeDtyp...  153 us

profile of v2, /device:TPU:33, one launch (start us, length us, event | category | flops | bytes accessed | tf_op | source)
XLA Modules:
  0.0 155.0 jit_solution(9690117171589806266)
XLA Ops:
  0.0 153.1 %shard_map.163 = bf16[1024,256]{1,0:T(8,128)(2,1)} custom-call(bf16[1024,256]{1,0:T(8,128)(2,1)} %bitcast.7, f32[1,2048]{1,0:T(1,128)} %bitcast.10, f32[128,128]{1,0:T(8,128)} %in_m.1, f32[1,128]{1,0:T(1,128)} %in_s.1, bf16[1,128,128]{2,1,0:T(8,128)(2,1)} %pool_m.1, f32[1,128]{1,0:T(1,128)} %pool_s.1, f32[128,128]{1,0:T(8,128)} %out_m.1, f32[1,128]{1,0:T(1,128)} %out_s.1, ...), custom_call_target="tpu_custom_call" | custom-call | tf_op jit(solution)/shard_map/pallas_call | solution.py:578
  153.1 1.9 %copy.19 = bf16[1,1024,256]{2,1,0:T(8,128)(2,1)} copy(bf16[1,1024,256]{2,1,0:T(8,128)(2,1)} %bitcast.6) | data formatting | bytes 1048576

commit v3 on v2

--- a/solution.py
+++ b/solution.py
@@ -13,15 +13,19 @@
 F32 = jnp.float32
 LANES = 128
 CORES = 2
+ROUTE = {
+    1: (0, 1), 15: (0, -1), 2: (0, 2), 14: (0, -2), 4: (0, 4), 12: (0, -4), 8: (0, 8),
+    5: (4, 1), 3: (4, -1), 6: (4, 2), 13: (12, 1), 11: (12, -1), 10: (12, -2), 9: (8, 1), 7: (8, -1),
+}
 
 
 class FeatureGather:
     TAGS = 13
     R0, R1, L1, L0, F0, F1, OWN, PL0, PL1, PR0, PR1, PO0, PO1 = range(13)
 
-    def __init__(self, buf, send, recv, chips, x, core):
+    def __init__(self, buf, send, recv, chips, x, core, base, count):
         self.buf, self.send, self.recv = buf, send, recv
-        self.half = buf.shape[1] // 2
+        self.base, self.half = base, count // 2
         at = lambda chip, c: lax.rem(chip, chips) * CORES + c
         other = 1 - core
         self.me, self.mate = at(x, core), at(x, other)
@@ -53,8 +57,8 @@
 
     def ref(self, block, part):
         if part is None:
-            return self.buf.at[block]
-        return self.buf.at[block, pl.ds(part * self.half, self.half)]
+            return self.buf.at[block, pl.ds(self.base, 2 * self.half)]
+        return self.buf.at[block, pl.ds(self.base + part * self.half, self.half)]
 
     def copy(self, tag, block, part, to):
         ref = self.ref(block, part)
@@ -85,9 +89,9 @@
     tok_in, mix_gain, in_m, in_s, pool_m, pool_s, out_m, out_s, ffn_gain,
     gate_m, gate_s, up_m, up_s, gate_t, up_t, down_m, down_s,
     out_ref,
-    tok, res, nf, io, inw, outg, outw, proj, pool, gu, par, lin, hid, dn, sums, far, near,
+    tok, res, nf, io, inw, outg, outw, proj, pool, gu, par, lin, edge, hid, dn, sums, far, near,
     load_sem, zsend, zrecv, gsend, grecv, osend, orecv, hsend, hrecv, dsend, drecv,
-    ysend, yrecv, fsend, frecv, rsend, rrecv,
+    ysend, yrecv, asend, arecv, xsend, xrecv, fsend, frecv, rsend, rrecv,
 ):
     z, me, group = lax.axis_index("fs"), lax.axis_index("tp"), lax.axis_index("grp")
     side = lax.rem(group, 2)
@@ -110,8 +114,11 @@
     load = pltpu.make_async_copy(tok_in, tok.at[me], load_sem)
     load.start()
 
-    io[z, 0:depth, :] = in_m[...].astype(BF16)
-    io[z, depth:, :] = (out_m[...] * out_s[...]).astype(BF16)
+    half = depth // 2
+    scaled_out = (out_m[...] * out_s[...]).astype(BF16)
+    for k in range(2):
+        io[z, k, 0:half, :] = in_m[k * half : (k + 1) * half, :].astype(BF16)
+        io[z, k, half:, :] = scaled_out[k * half : (k + 1) * half]
 
     def packed(g_ref, u_ref):
         for j in range(full):
@@ -139,32 +146,32 @@
         return 0
 
     lax.fori_loop(0, zn, clear, 0)
-    lin[0:8, :] = jnp.zeros((8, lin.shape[1]), F32)
+    edge[...] = jnp.zeros(edge.shape, F32)
     load.wait()
 
     barrier = pltpu.get_barrier_semaphore()
-    for to in (zleft, zright):
-        pl.semaphore_signal(barrier, inc=1, device_id={"fs": to}, device_id_type=MESH)
+    reach = sorted({o for _, o in ROUTE.values()})
+    for o in reach:
+        pl.semaphore_signal(barrier, inc=1, device_id={"fs": lax.rem(z + o + zn, zn)}, device_id_type=MESH)
     for j in range(1, tn):
         pl.semaphore_signal(barrier, inc=1, device_id={"tp": lax.rem(me + j, tn)}, device_id_type=MESH)
     pl.semaphore_signal(barrier, inc=1, device_id={"grp": twin}, device_id_type=MESH)
-    pl.semaphore_wait(barrier, tn + 2)
-
-    def io_part(slot, part):
-        n = 2 * depth
-        if part is None:
-            return io.at[slot]
-        return io.at[slot, pl.ds(part * (n // 2), n // 2)]
-
-    half = depth // 2
-    cut = half // 2
-
-    def gu_rows(b, slot, whose, part):
-        a, m = (b * cut, cut) if part is None else (b * cut + part * (cut // 2), cut // 2)
-        return gu.at[pl.ds(pl.multiple_of(slot * depth + whose * half + a, 16), m)]
-
-    def gu_part(b):
-        return lambda slot, part: gu_rows(b, slot, side, part)
+    pl.semaphore_wait(barrier, tn + len(reach))
+
+    shared = 3 * depth // 8
+    common = depth - 2 * shared
+
+    def gu_ref(slot, a, m):
+        return gu.at[pl.ds(pl.multiple_of(slot * depth + a, 16), m)]
+
+    def gu_shared(slot, part, whose):
+        n = 2 * shared // 3
+        a, m = ((0, shared), (0, n), (n, shared - n))[0 if part is None else part + 1]
+        return gu_ref(slot, whose * shared + a, m)
+
+    def gu_common(slot, part):
+        a, m = (0, common) if part is None else (part * (common // 2), common // 2)
+        return gu_ref(slot, 2 * shared + a, m)
 
     def dn_part(r0, n):
         def at(slot, part):
@@ -173,8 +180,11 @@
 
         return at
 
-    lanes = [io_part, gu_part(0), gu_part(1), dn_part(0, ff // 2), dn_part(ff // 2, ff // 2)]
-    A, B1, B2, C1, C2 = range(5)
+    lanes = [
+        lambda slot, part: gu_shared(slot, part, side), gu_common,
+        dn_part(0, ff // 2), dn_part(ff // 2, ff // 2),
+    ]
+    B1, B2, C1, C2 = range(4)
 
     def zslot(d, s):
         return lax.rem(z + zn + (s if d else -s), zn)
@@ -211,10 +221,10 @@
         if isinstance(s, int) and s == hops:
             handed(i, 0, s)
 
-    def ycopy(b, d, s, whose):
-        ref = gu_rows(b, zslot(d, s), whose, None)
-        return pltpu.make_async_remote_copy(
-            ref, ref, ysend.at[b, d, s], yrecv.at[b, d, s], device_id={"grp": twin}, device_id_type=MESH
+    def ycopy(d, s, whose):
+        ref = gu_shared(zslot(d, s), None, whose)
+        return pltpu.make_async_remote_copy(
+            ref, ref, ysend.at[d, s], yrecv.at[d, s], device_id={"grp": twin}, device_id_type=MESH
         )
 
     def hand(c, d, s, which):
@@ -226,26 +236,61 @@
     def ocopy(slot, src):
         owner = lax.div(slot, per)
         return pltpu.make_async_remote_copy(
-            io.at[slot, pl.ds(depth, depth)], outg.at[src, lax.rem(slot, per)],
+            io.at[slot, pl.ds(0, 2), pl.ds(half, half)], outg.at[src, lax.rem(slot, per)],
             osend.at[slot], orecv.at[src, lax.rem(slot, per)],
             device_id={"tp": owner}, device_id_type=MESH,
         )
 
     def handed(i, d, s):
-        if i == A:
-            slot = zslot(d, s)
-
+        if i == B1:
+            if not (isinstance(s, int) and s == 1):
+                ycopy(d, s, side).start()
+        elif i in (C1, C2):
+            hand(i - C1, d, s, core).start()
+
+    def acopy(off, sending):
+        behind, o = ROUTE[off]
+        slot = lax.rem(z - (behind if sending else off) + zn, zn)
+        ref = io.at[slot, side]
+        return pltpu.make_async_remote_copy(
+            ref, ref, asend.at[off], arecv.at[off],
+            device_id={"fs": lax.rem(z + o + zn, zn)}, device_id_type=MESH,
+        )
+
+    def across(off, whose):
+        ref = io.at[lax.rem(z - off + zn, zn), whose]
+        return pltpu.make_async_remote_copy(
+            ref, ref, xsend.at[off], xrecv.at[off], device_id={"grp": twin}, device_id_type=MESH
+        )
+
+    def aput(behind):
+        for off, (b, _) in ROUTE.items():
+            if b == behind:
+                acopy(off, True).start()
+
+    def agot(*offs):
+        for off in offs:
+            acopy(off, False).wait_recv()
+            if off in (4, 12, 8):
+                aput(off)
+            across(off, side).start()
+
+    def a_all():
+        for off in ROUTE:
+            across(off, 1 - side).wait_recv()
+
+        def body(slot, _):
             @pl.when(lax.div(slot, per) != me)
             def _():
                 ocopy(slot, me).start()
-        elif i in (B1, B2):
-            ycopy(i - B1, d, s, side).start()
-        else:
-            hand(i - C1, d, s, core).start()
-
-
-    def each_arrival(fn):
-        fn(0, 0)
+
+            return 0
+
+        lax.fori_loop(0, zn, body, 0)
+
+    def each_arrival(fn, own=True):
+        if own:
+            fn(0, 0)
 
         def body(s, _):
             fn(0, s)
@@ -256,22 +301,15 @@
         fn(0, hops)
 
     def steps():
-        for s in range(1, hops + 1):
-            tick(A, s)
-            if s == hops - 1:
-                zopen(B2)
-            tick(B1, s)
-            if s == hops - 1:
-                zopen(C1)
-            yield
-        for s in range(1, hops + 1):
-            tick(B2, s)
-            tick(C1, s)
-            if s == hops - 2:
-                zopen(C2)
-            if s > hops - 2:
-                tick(C2, s + 2 - hops)
-            yield
+        for first, second in ((B1, B2), (C1, C2)):
+            for s in range(1, hops + 1):
+                tick(first, s)
+                if first == B1 and s == hops - 1:
+                    zopen(C1)
+                tick(second, s)
+                if first == B1 and s == hops - 1:
+                    zopen(C2)
+                yield
 
     ring = steps()
 
@@ -280,15 +318,19 @@
             next(ring)
 
     gathers = [
-        FeatureGather(buf, gsend.at[k], grecv.at[k], chips, x, core) for k, buf in enumerate((tok, pool, res))
+        FeatureGather(buf, gsend.at[k], grecv.at[k], chips, x, core, base, count)
+        for k, (buf, base, count) in enumerate(
+            ((tok, 0, length), (pool, 0, length), (res, 0, length // 2), (res, length // 2, length // 2))
+        )
     ]
-    g_tok, g_pool, g_res = gathers
+    g_tok, g_pool, g_first, g_second = gathers
     G = FeatureGather
 
-    zopen(A)
+    aput(0)
     zopen(B1)
+    zopen(B2)
     g_tok.start()
-    for i in (A, B1, B2, C1, C2):
+    for i in (C1, C2):
         handed(i, 0, 0)
 
     def norm(buf, gain_ref, lo, hi):
@@ -309,24 +351,30 @@
 
         lax.fori_loop(lo // rows, hi // rows, body, 0)
 
-    go(2)
+    agot(1, 15, 2, 14)
+    agot(4, 12)
     g_tok.arrive(G.R0, G.L1)
-    go(1)
+    agot(8)
+    go(1)
+    agot(5, 3, 6, 13, 11, 10)
+    agot(9, 7)
+    for d in range(2):
+        ycopy(d, 1, side).start()
     g_tok.arrive(G.R1, G.L0)
-    go(2)
+    go(1)
+    a_all()
     g_tok.arrive(G.F0, G.F1)
     g_tok.finish()
     part = length // 4
     norm(tok, mix_gain, 0, part)
-    go(1)
     norm(tok, mix_gain, part, 2 * part)
     norm(tok, mix_gain, 2 * part, 3 * part)
-    go(1)
     norm(tok, mix_gain, 3 * part, length)
     go(1)
 
     for k in range(zn):
-        inw[k * depth : (k + 1) * depth, :] = io[k, 0:depth, :]
+        for h in range(2):
+            inw[k * depth + h * half : k * depth + (h + 1) * half, :] = io[k, h, 0:half, :]
     tile = length // 4
 
     def project(i, _):
@@ -364,10 +412,12 @@
 
     others(lambda p, k: ocopy(me * per + k, p).wait_recv())
     for k in range(per):
-        outg[me, k] = io[me * per + k, depth:, :]
+        outg[me, k] = io[me * per + k, :, half:, :]
     for p in range(tn):
         for k in range(per):
-            outw[p * chan : (p + 1) * chan, k * ocols : (k + 1) * ocols] = outg[p, k]
+            for h in range(2):
+                rows = slice(p * chan + h * half, p * chan + (h + 1) * half)
+                outw[rows, k * ocols : (k + 1) * ocols] = outg[p, k, h]
     go(1)
     g_pool.arrive(G.R1, G.L0)
     g_pool.arrive(G.F0, G.F1)
@@ -381,32 +431,42 @@
         res[me, r, :] = (tok[me, r, :].astype(F32) + v).astype(BF16)
         return 0
 
-    lax.fori_loop(0, 4, mix, 0)
-    g_res.start()
-    go(2)
-    g_res.arrive(G.R0, G.L1)
-    go(1)
-    g_res.arrive(G.R1, G.L0)
-    go(1)
-    g_res.arrive(G.F0, G.F1)
-    g_res.finish()
+    lax.fori_loop(0, 2, mix, 0)
+    g_first.start()
+    lax.fori_loop(2, 4, mix, 0)
+    go(1)
+    g_first.arrive(G.R0, G.L1)
+    g_second.start()
+    go(1)
+    g_first.arrive(G.R1, G.L0)
+    g_first.arrive(G.F0, G.F1)
+    go(1)
+    g_first.finish()
     norm(res, ffn_gain, 0, length // 2)
-    go(1)
-    norm(res, ffn_gain, length // 2, length)
-    for b in range(2):
-        each_arrival(lambda d, s, b=b: ycopy(b, d, s, 1 - side).wait_recv())
-
-    taps = lin.shape[0] - length
-
-    def tile_product(at, n):
+
+    def both_down(s):
+        tick(C1, s)
+        tick(C2, s)
+
+    g_second.arrive(G.R0, G.L1)
+    both_down(2)
+    each_arrival(lambda d, s: ycopy(d, s, 1 - side).wait_recv(), own=False)
+
+    side_rows = length // 2
+    taps = lin.shape[0] - side_rows
+
+    def tile_product(h, j, at, n):
+        lin[0:taps, 0:n] = edge[j, :, 0:n]
+
         def body(i, _):
-            r = pl.ds(pl.multiple_of(i * tile, tile), tile)
+            r = pl.ds(pl.multiple_of(h * side_rows + i * tile, tile), tile)
             v = jnp.dot(nf[r, :], gu[:, pl.ds(at, n)], preferred_element_type=F32)
             v = (v * par[0:1, pl.ds(at, n)]).astype(BF16).astype(F32)
             lin[pl.ds(pl.multiple_of(taps + i * tile, 8), tile), 0:n] = v
             return 0
 
-        lax.fori_loop(0, 4, body, 0)
+        lax.fori_loop(0, side_rows // tile, body, 0)
+        edge[j, :, 0:n] = lin[side_rows:, 0:n]
 
     chunk = 64
 
@@ -420,59 +480,90 @@
     def silu(g):
         return g / (1.0 + jnp.exp(-g))
 
-    def hcopy(j, which):
-        ref = hid.at[which, j]
-        return pltpu.make_async_remote_copy(
-            ref, ref, hsend.at[j], hrecv.at[j], device_id={"tp": mate}, device_id_type=MESH
-        )
-
-    def column(j):
+    def hcopy(h, j, which):
+        ref = hid.at[which, j, pl.ds(h * side_rows, side_rows)]
+        return pltpu.make_async_remote_copy(
+            ref, ref, hsend.at[h, j], hrecv.at[h, j], device_id={"tp": mate}, device_id_type=MESH
+        )
+
+    def store_rows(h, i):
+        return pl.ds(pl.multiple_of(h * side_rows + i * chunk, chunk), chunk)
+
+    def column(h, j):
         at = pl.multiple_of(j * 2 * LANES, 2 * LANES)
-        tile_product(at, 2 * LANES)
+        tile_product(h, j, at, 2 * LANES)
 
         def body(i, _):
-            r = pl.ds(pl.multiple_of(i * chunk, chunk), chunk)
-            h = silu(convolved(i, at, 0)) * convolved(i, at, LANES)
-            hid[core, j, r, :] = h.astype(BF16)
-            return 0
-
-        lax.fori_loop(0, length // chunk, body, 0)
-        hcopy(j, core).start()
-
-    early = 3
-
-    def some_columns(j, _):
-        column(j)
-        tick(C2, j + early)
-        return 0
-
-    lax.fori_loop(0, full - 1, some_columns, 0)
-    column(full - 1)
-    tick(C2, full - 1 + early)
+            v = silu(convolved(i, at, 0)) * convolved(i, at, LANES)
+            hid[core, j, store_rows(h, i), :] = v.astype(BF16)
+            return 0
+
+        lax.fori_loop(0, side_rows // chunk, body, 0)
+        hcopy(h, j, core).start()
+
     last = 2 * full * LANES
-    tile_product(last, LANES)
     lane = lax.broadcasted_iota(jnp.int32, (chunk, LANES), 1)
 
-    def narrow(i, _):
-        r = pl.ds(pl.multiple_of(i * chunk, chunk), chunk)
-        y = convolved(i, last, 0)
-        h = jnp.where(lane < tail, silu(y) * pltpu.roll(y, LANES - tail, 1), 0.0)
-        hid[core, full, r, :] = h.astype(BF16)
-        return 0
-
-    lax.fori_loop(0, length // chunk, narrow, 0)
-    hcopy(full, core).start()
-    tick(C2, hops)
+    def narrow_column(h):
+        tile_product(h, full, last, LANES)
+
+        def body(i, _):
+            y = convolved(i, last, 0)
+            v = jnp.where(lane < tail, silu(y) * pltpu.roll(y, LANES - tail, 1), 0.0)
+            hid[core, full, store_rows(h, i), :] = v.astype(BF16)
+            return 0
+
+        lax.fori_loop(0, side_rows // chunk, body, 0)
+        hcopy(h, full, core).start()
+
+    def feed(h, after):
+        def body(j, _):
+            column(h, j)
+            after(j)
+            return 0
+
+        lax.fori_loop(0, full, body, 0)
+        narrow_column(h)
+
+    def after_first(j):
+        @pl.when(j == 0)
+        def _():
+            g_second.arrive(G.R1, G.L0)
+
+        @pl.when(j == 1)
+        def _():
+            both_down(3)
+
+        @pl.when(j == 2)
+        def _():
+            g_second.arrive(G.F0, G.F1)
+
+        @pl.when(j == 4)
+        def _():
+            both_down(4)
+
+    def after_second(j):
+        @pl.when(j == 2)
+        def _():
+            both_down(6)
+
+    feed(0, after_first)
+    g_second.finish()
+    norm(res, ffn_gain, side_rows, length)
+    both_down(5)
+    feed(1, after_second)
+    both_down(hops - 1)
+    both_down(hops)
 
     for j in range(full + 1):
-        hcopy(j, other).wait_recv()
+        for h in range(2):
+            hcopy(h, j, other).wait_recv()
     for c in range(2):
         each_arrival(lambda d, s, c=c: hand(c, d, s, other).wait_recv())
 
     at_chip = lambda m: lax.rem(m, chips) * CORES + core
     FAR, RIGHT, LEFT, OWN = range(4)
     owner_of = (x + 2, x + 1, x + chips - 1, x)
-    side_rows = length // 2
 
     def down(which, h, extra=None):
         m = lax.rem(owner_of[which], chips)
@@ -544,7 +635,8 @@
     for g in gathers:
         g.drain()
     for j in range(full + 1):
-        hcopy(j, core).wait_send()
+        for h in range(2):
+            hcopy(h, j, core).wait_send()
 
     def outs_left(slot, _):
         @pl.when(lax.div(slot, per) != me)
@@ -554,8 +646,11 @@
         return 0
 
     lax.fori_loop(0, zn, outs_left, 0)
+    each_arrival(lambda d, s: ycopy(d, s, side).wait_send(), own=False)
+    for off in ROUTE:
+        across(off, side).wait_send()
+        acopy(off, True).wait_send()
     for b in range(2):
-        each_arrival(lambda d, s, b=b: ycopy(b, d, s, side).wait_send())
         each_arrival(lambda d, s, b=b: hand(b, d, s, core).wait_send())
     for h in range(2):
         far_copy(h).wait_send()
@@ -570,7 +665,7 @@
     ff = gate_m.shape[1]
     ocols = out_m.shape[1]
     per = width // ocols
-    assert ff % LANES == LANES // 2 and per == 2 and chan == LANES and tn == 4 * CORES and gn % 2 == 0
+    assert ff % LANES == LANES // 2 and per == 2 and chan == LANES and tn == 4 * CORES and gn % 2 == 0 and zn == 16
     tiles = ff // LANES + 1
     hops = zn // 2
     dma = pltpu.SemaphoreType.DMA
@@ -584,27 +679,29 @@
             pltpu.VMEM((tn, length, width), BF16),
             pltpu.VMEM((tn, length, width), BF16),
             pltpu.VMEM((length, tn * width), BF16),
-            pltpu.VMEM((zn, 2 * depth, chan), BF16),
+            pltpu.VMEM((zn, 2, depth, chan), BF16),
             pltpu.VMEM((zn * depth, chan), BF16),
-            pltpu.VMEM((tn, per, chan, ocols), BF16),
+            pltpu.VMEM((tn, per, 2, chan // 2, ocols), BF16),
             pltpu.VMEM((tn * chan, width), BF16),
             pltpu.VMEM((length, chan), F32),
             pltpu.VMEM((tn, length, chan), BF16),
             pltpu.VMEM((zn * depth, 2 * ff), BF16),
             pltpu.VMEM((8, 2 * ff), F32),
-            pltpu.VMEM((length + 8, 2 * LANES), F32),
+            pltpu.VMEM((length // 2 + 8, 2 * LANES), F32),
+            pltpu.VMEM((tiles, 8, 2 * LANES), F32),
             pltpu.VMEM((CORES, tiles, length, LANES), BF16),
             pltpu.VMEM((CORES, zn, tiles * LANES, ocols), BF16),
             pltpu.VMEM((4, length, width), BF16),
             pltpu.VMEM((2, length // 2, width), BF16),
             pltpu.VMEM((2, length, width), BF16),
             dma,
-            dma((5, 2)), dma((5, 2, hops)),
-            dma((3, FeatureGather.TAGS)), dma((3, FeatureGather.TAGS)),
+            dma((4, 2)), dma((4, 2, hops)),
+            dma((4, FeatureGather.TAGS)), dma((4, FeatureGather.TAGS)),
             dma((zn,)), dma((tn, per)),
-            dma((tiles,)), dma((tiles,)),
+            dma((2, tiles)), dma((2, tiles)),
             dma((2, 2, hops + 1)), dma((2, 2, hops + 1)),
-            dma((2, 2, hops + 1)), dma((2, 2, hops + 1)),
+            dma((2, hops + 1)), dma((2, hops + 1)),
+            dma((zn,)), dma((zn,)), dma((zn,)), dma((zn,)),
             dma((2,)), dma((2,)),
             dma((2, 2)), dma((2, 2)),
         ],

time: 155 us -> 149 us (0.961)
  Pallas kernels: 153 us -> 147 us
    pallas_call x1, Pallas kernels: 153 us -> 147 us  [layer(): pl.pallas_call(functools.partial(kernel, zn, tn), out_shape=jax.ShapeDtyp...]
where the time goes in v3:
time: 149 us; the launch traced here: 148 us
  Pallas kernels  147 us (99%)
  local copies, waits for them, and re-layouts  1.87 us (1%)
    pallas_call x1, Pallas kernels, layer(): pl.pallas_call(functools.partial(kernel, zn, tn), out_shape=jax.ShapeDtyp...  147 us

profile of v3, /device:TPU:33, one launch (start us, length us, event | category | flops | bytes accessed | tf_op | source)
XLA Modules:
  0.0 148.4 jit_solution(8142050468727389891)
XLA Ops:
  0.0 146.5 %shard_map.163 = bf16[1024,256]{1,0:T(8,128)(2,1)} custom-call(bf16[1024,256]{1,0:T(8,128)(2,1)} %bitcast.7, f32[1,2048]{1,0:T(1,128)} %bitcast.10, f32[128,128]{1,0:T(8,128)} %in_m.1, f32[1,128]{1,0:T(1,128)} %in_s.1, bf16[1,128,128]{2,1,0:T(8,128)(2,1)} %pool_m.1, f32[1,128]{1,0:T(1,128)} %pool_s.1, f32[128,128]{1,0:T(8,128)} %out_m.1, f32[1,128]{1,0:T(1,128)} %out_s.1, ...), custom_call_target="tpu_custom_call" | custom-call | tf_op jit(solution)/shard_map/pallas_call | solution.py:673
  146.5 1.9 %copy.19 = bf16[1,1024,256]{2,1,0:T(8,128)(2,1)} copy(bf16[1,1024,256]{2,1,0:T(8,128)(2,1)} %bitcast.6) | data formatting | bytes 1048576

commit v4 on v3

--- a/solution.py
+++ b/solution.py
@@ -14,9 +14,11 @@
 LANES = 128
 CORES = 2
 ROUTE = {
-    1: (0, 1), 15: (0, -1), 2: (0, 2), 14: (0, -2), 4: (0, 4), 12: (0, -4), 8: (0, 8),
+    1: (0, 1), 15: (0, -1), 2: (0, 2), 14: (0, -2), 4: (0, 4), 12: (0, -4),
     5: (4, 1), 3: (4, -1), 6: (4, 2), 13: (12, 1), 11: (12, -1), 10: (12, -2), 9: (8, 1), 7: (8, -1),
 }
+QUARTER, OPPOSITE = 4, 8
+BEHIND = (*ROUTE, OPPOSITE)
 
 
 class FeatureGather:
@@ -91,7 +93,7 @@
     out_ref,
     tok, res, nf, io, inw, outg, outw, proj, pool, gu, par, lin, edge, hid, dn, sums, far, near,
     load_sem, zsend, zrecv, gsend, grecv, osend, orecv, hsend, hrecv, dsend, drecv,
-    ysend, yrecv, asend, arecv, xsend, xrecv, fsend, frecv, rsend, rrecv,
+    ysend, yrecv, asend, arecv, esend, erecv, xsend, xrecv, fsend, frecv, rsend, rrecv,
 ):
     z, me, group = lax.axis_index("fs"), lax.axis_index("tp"), lax.axis_index("grp")
     side = lax.rem(group, 2)
@@ -110,6 +112,14 @@
     full = ff // LANES
     tail = ff - full * LANES
     per = width // ocols
+
+    barrier = pltpu.get_barrier_semaphore()
+    reach = sorted({o for _, o in ROUTE.values()})
+    for o in reach:
+        pl.semaphore_signal(barrier, inc=1, device_id={"fs": lax.rem(z + o + zn, zn)}, device_id_type=MESH)
+    for j in range(1, tn):
+        pl.semaphore_signal(barrier, inc=1, device_id={"tp": lax.rem(me + j, tn)}, device_id_type=MESH)
+    pl.semaphore_signal(barrier, inc=1, device_id={"grp": twin}, device_id_type=MESH)
 
     load = pltpu.make_async_copy(tok_in, tok.at[me], load_sem)
     load.start()
@@ -149,13 +159,6 @@
     edge[...] = jnp.zeros(edge.shape, F32)
     load.wait()
 
-    barrier = pltpu.get_barrier_semaphore()
-    reach = sorted({o for _, o in ROUTE.values()})
-    for o in reach:
-        pl.semaphore_signal(barrier, inc=1, device_id={"fs": lax.rem(z + o + zn, zn)}, device_id_type=MESH)
-    for j in range(1, tn):
-        pl.semaphore_signal(barrier, inc=1, device_id={"tp": lax.rem(me + j, tn)}, device_id_type=MESH)
-    pl.semaphore_signal(barrier, inc=1, device_id={"grp": twin}, device_id_type=MESH)
     pl.semaphore_wait(barrier, tn + len(reach))
 
     shared = 3 * depth // 8
@@ -264,19 +267,35 @@
         )
 
     def aput(behind):
-        for off, (b, _) in ROUTE.items():
+        for off, (b, _) in sorted(ROUTE.items(), key=lambda r: r[0] not in (QUARTER, -QUARTER % zn)):
             if b == behind:
                 acopy(off, True).start()
 
     def agot(*offs):
         for off in offs:
             acopy(off, False).wait_recv()
-            if off in (4, 12, 8):
+            if off in (QUARTER, -QUARTER % zn):
+                opposite(int(off != QUARTER), True).start()
                 aput(off)
             across(off, side).start()
 
+    def opposite(k, sending):
+        o = -QUARTER if k else QUARTER
+        slot = lax.rem(z + (-o if sending else OPPOSITE) + zn, zn)
+        ref = io.at[slot, side, pl.ds(k * half, half)]
+        return pltpu.make_async_remote_copy(
+            ref, ref, esend.at[k], erecv.at[k],
+            device_id={"fs": lax.rem(z + o + zn, zn)}, device_id_type=MESH,
+        )
+
+    def opposite_got():
+        for k in range(2):
+            opposite(k, False).wait_recv()
+        aput(OPPOSITE)
+        across(OPPOSITE, side).start()
+
     def a_all():
-        for off in ROUTE:
+        for off in BEHIND:
             across(off, 1 - side).wait_recv()
 
         def body(slot, _):
@@ -351,10 +370,10 @@
 
         lax.fori_loop(lo // rows, hi // rows, body, 0)
 
+    agot(4, 12)
     agot(1, 15, 2, 14)
-    agot(4, 12)
     g_tok.arrive(G.R0, G.L1)
-    agot(8)
+    opposite_got()
     go(1)
     agot(5, 3, 6, 13, 11, 10)
     agot(9, 7)
@@ -368,9 +387,9 @@
     part = length // 4
     norm(tok, mix_gain, 0, part)
     norm(tok, mix_gain, part, 2 * part)
+    go(1)
     norm(tok, mix_gain, 2 * part, 3 * part)
     norm(tok, mix_gain, 3 * part, length)
-    go(1)
 
     for k in range(zn):
         for h in range(2):
@@ -421,7 +440,6 @@
     go(1)
     g_pool.arrive(G.R1, G.L0)
     g_pool.arrive(G.F0, G.F1)
-    go(1)
     g_pool.finish()
 
     def mix(i, _):
@@ -434,7 +452,7 @@
     lax.fori_loop(0, 2, mix, 0)
     g_first.start()
     lax.fori_loop(2, 4, mix, 0)
-    go(1)
+    go(2)
     g_first.arrive(G.R0, G.L1)
     g_second.start()
     go(1)
@@ -543,16 +561,19 @@
             both_down(4)
 
     def after_second(j):
-        @pl.when(j == 2)
+        @pl.when(j == 1)
         def _():
             both_down(6)
+
+        @pl.when(j == 4)
+        def _():
+            both_down(hops - 1)
 
     feed(0, after_first)
     g_second.finish()
     norm(res, ffn_gain, side_rows, length)
     both_down(5)
     feed(1, after_second)
-    both_down(hops - 1)
     both_down(hops)
 
     for j in range(full + 1):
@@ -647,9 +668,12 @@
 
     lax.fori_loop(0, zn, outs_left, 0)
     each_arrival(lambda d, s: ycopy(d, s, side).wait_send(), own=False)
+    for off in BEHIND:
+        across(off, side).wait_send()
     for off in ROUTE:
-        across(off, side).wait_send()
         acopy(off, True).wait_send()
+    for k in range(2):
+        opposite(k, True).wait_send()
     for b in range(2):
         each_arrival(lambda d, s, b=b: hand(b, d, s, core).wait_send())
     for h in range(2):
@@ -665,7 +689,7 @@
     ff = gate_m.shape[1]
     ocols = out_m.shape[1]
     per = width // ocols
-    assert ff % LANES == LANES // 2 and per == 2 and chan == LANES and tn == 4 * CORES and gn % 2 == 0 and zn == 16
+    assert ff % LANES == LANES // 2 and per == 2 and chan == LANES and tn == 4 * CORES and gn % 2 == 0 and zn == 2 * OPPOSITE
     tiles = ff // LANES + 1
     hops = zn // 2
     dma = pltpu.SemaphoreType.DMA
@@ -701,7 +725,7 @@
             dma((2, tiles)), dma((2, tiles)),
             dma((2, 2, hops + 1)), dma((2, 2, hops + 1)),
             dma((2, hops + 1)), dma((2, hops + 1)),
-            dma((zn,)), dma((zn,)), dma((zn,)), dma((zn,)),
+            dma((zn,)), dma((zn,)), dma((2,)), dma((2,)), dma((zn,)), dma((zn,)),
             dma((2,)), dma((2,)),
             dma((2, 2)), dma((2, 2)),
         ],

time: 149 us -> 147 us (0.987)
  Pallas kernels: 147 us -> 145 us
    pallas_call x1, Pallas kernels: 147 us -> 145 us  [layer(): pl.pallas_call(functools.partial(kernel, zn, tn), out_shape=jax.ShapeDtyp...]
where the time goes in v4:
time: 147 us
  Pallas kernels  145 us (99%)
  local copies, waits for them, and re-layouts  1.87 us (1%)
    pallas_call x1, Pallas kernels, layer(): pl.pallas_call(functools.partial(kernel, zn, tn), out_shape=jax.ShapeDtyp...  145 us

profile of v4, /device:TPU:33, one launch (start us, length us, event | category | flops | bytes accessed | tf_op | source)
XLA Modules:
  0.0 146.7 jit_solution(12729077343506834604)
XLA Ops:
  0.0 144.8 %shard_map.163 = bf16[1024,256]{1,0:T(8,128)(2,1)} custom-call(bf16[1024,256]{1,0:T(8,128)(2,1)} %bitcast.7, f32[1,2048]{1,0:T(1,128)} %bitcast.10, f32[128,128]{1,0:T(8,128)} %in_m.1, f32[1,128]{1,0:T(1,128)} %in_s.1, bf16[1,128,128]{2,1,0:T(8,128)(2,1)} %pool_m.1, f32[1,128]{1,0:T(1,128)} %pool_s.1, f32[128,128]{1,0:T(8,128)} %out_m.1, f32[1,128]{1,0:T(1,128)} %out_s.1, ...), custom_call_target="tpu_custom_call" | custom-call | tf_op jit(solution)/shard_map/pallas_call | solution.py:697
  144.8 1.9 %copy.19 = bf16[1,1024,256]{2,1,0:T(8,128)(2,1)} copy(bf16[1,1024,256]{2,1,0:T(8,128)(2,1)} %bitcast.6) | data formatting | bytes 1048576

commit v5 on v4

--- a/solution.py
+++ b/solution.py
@@ -86,6 +86,11 @@
             self.copy(tag, *self.out[tag]).wait_send()
 
 
+def down_cuts(ff):
+    n = (ff // 3 + 31) // 32 * 32
+    return (0, n), (n, n), (2 * n, ff - 2 * n)
+
+
 def kernel(
     zn, tn,
     tok_in, mix_gain, in_m, in_s, pool_m, pool_s, out_m, out_s, ffn_gain,
@@ -185,9 +190,9 @@
 
     lanes = [
         lambda slot, part: gu_shared(slot, part, side), gu_common,
-        dn_part(0, ff // 2), dn_part(ff // 2, ff // 2),
+        *(dn_part(*c) for c in down_cuts(ff)),
     ]
-    B1, B2, C1, C2 = range(4)
+    B1, B2, *C = range(len(lanes))
 
     def zslot(d, s):
         return lax.rem(z + zn + (s if d else -s), zn)
@@ -231,7 +236,7 @@
         )
 
     def hand(c, d, s, which):
-        ref = dn.at[which, zslot(d, s), pl.ds(c * (ff // 2), ff // 2)]
+        ref = dn.at[which, zslot(d, s), pl.ds(*down_cuts(ff)[c])]
         return pltpu.make_async_remote_copy(
             ref, ref, dsend.at[c, d, s], drecv.at[c, d, s], device_id={"tp": mate}, device_id_type=MESH
         )
@@ -248,8 +253,8 @@
         if i == B1:
             if not (isinstance(s, int) and s == 1):
                 ycopy(d, s, side).start()
-        elif i in (C1, C2):
-            hand(i - C1, d, s, core).start()
+        elif i in C:
+            hand(i - C[0], d, s, core).start()
 
     def acopy(off, sending):
         behind, o = ROUTE[off]
@@ -320,15 +325,22 @@
         fn(0, hops)
 
     def steps():
-        for first, second in ((B1, B2), (C1, C2)):
-            for s in range(1, hops + 1):
-                tick(first, s)
-                if first == B1 and s == hops - 1:
-                    zopen(C1)
-                tick(second, s)
-                if first == B1 and s == hops - 1:
-                    zopen(C2)
-                yield
+        for s in range(1, hops + 1):
+            tick(B1, s)
+            if s == hops - 1:
+                zopen(C[0])
+            tick(B2, s)
+            if s == hops - 1:
+                for i in C[1:]:
+                    zopen(i)
+            yield
+        for s in range(1, hops + 1):
+            all_down(s)
+            yield
+
+    def all_down(s):
+        for i in C:
+            tick(i, s)
 
     ring = steps()
 
@@ -349,7 +361,7 @@
     zopen(B1)
     zopen(B2)
     g_tok.start()
-    for i in (C1, C2):
+    for i in C:
         handed(i, 0, 0)
 
     def norm(buf, gain_ref, lo, hi):
@@ -462,12 +474,8 @@
     g_first.finish()
     norm(res, ffn_gain, 0, length // 2)
 
-    def both_down(s):
-        tick(C1, s)
-        tick(C2, s)
-
     g_second.arrive(G.R0, G.L1)
-    both_down(2)
+    all_down(2)
     each_arrival(lambda d, s: ycopy(d, s, 1 - side).wait_recv(), own=False)
 
     side_rows = length // 2
@@ -543,43 +551,43 @@
         lax.fori_loop(0, full, body, 0)
         narrow_column(h)
 
+    def one_lane(j, start):
+        for k in range(full):
+
+            @pl.when(j == k)
+            def _(k=k):
+                tick(C[(start + k) % len(C)], (start + k) // len(C))
+
     def after_first(j):
         @pl.when(j == 0)
         def _():
             g_second.arrive(G.R1, G.L0)
 
-        @pl.when(j == 1)
-        def _():
-            both_down(3)
-
         @pl.when(j == 2)
         def _():
             g_second.arrive(G.F0, G.F1)
 
-        @pl.when(j == 4)
-        def _():
-            both_down(4)
+        one_lane(j, 3 * len(C) + 1)
 
     def after_second(j):
-        @pl.when(j == 1)
-        def _():
-            both_down(6)
-
-        @pl.when(j == 4)
-        def _():
-            both_down(hops - 1)
-
+        one_lane(j, 6 * len(C) + 1)
+
+    tick(C[0], 3)
     feed(0, after_first)
+    tick(C[0], 5)
     g_second.finish()
-    norm(res, ffn_gain, side_rows, length)
-    both_down(5)
+    tick(C[1], 5)
+    norm(res, ffn_gain, side_rows, side_rows + side_rows // 2)
+    tick(C[2], 5)
+    norm(res, ffn_gain, side_rows + side_rows // 2, length)
+    tick(C[0], 6)
     feed(1, after_second)
-    both_down(hops)
+    all_down(hops)
 
     for j in range(full + 1):
         for h in range(2):
             hcopy(h, j, other).wait_recv()
-    for c in range(2):
+    for c in range(len(C)):
         each_arrival(lambda d, s, c=c: hand(c, d, s, other).wait_recv())
 
     at_chip = lambda m: lax.rem(m, chips) * CORES + core
@@ -674,8 +682,8 @@
         acopy(off, True).wait_send()
     for k in range(2):
         opposite(k, True).wait_send()
-    for b in range(2):
-        each_arrival(lambda d, s, b=b: hand(b, d, s, core).wait_send())
+    for c in range(len(C)):
+        each_arrival(lambda d, s, c=c: hand(c, d, s, core).wait_send())
     for h in range(2):
         far_copy(h).wait_send()
         near_copy(RIGHT, h).wait_send()
@@ -719,11 +727,11 @@
             pltpu.VMEM((2, length // 2, width), BF16),
             pltpu.VMEM((2, length, width), BF16),
             dma,
-            dma((4, 2)), dma((4, 2, hops)),
+            dma((5, 2)), dma((5, 2, hops)),
             dma((4, FeatureGather.TAGS)), dma((4, FeatureGather.TAGS)),
             dma((zn,)), dma((tn, per)),
             dma((2, tiles)), dma((2, tiles)),
-            dma((2, 2, hops + 1)), dma((2, 2, hops + 1)),
+            dma((3, 2, hops + 1)), dma((3, 2, hops + 1)),
             dma((2, hops + 1)), dma((2, hops + 1)),
             dma((zn,)), dma((zn,)), dma((2,)), dma((2,)), dma((zn,)), dma((zn,)),
             dma((2,)), dma((2,)),

time: 147 us -> 146 us (level)
  no operation moved by 1% of the time
where the time goes in v5:
time: 146 us; the launch traced here: 145 us
  Pallas kernels  144 us (99%)
  local copies, waits for them, and re-layouts  1.87 us (1%)
    pallas_call x1, Pallas kernels, layer(): pl.pallas_call(functools.partial(kernel, zn, tn), out_shape=jax.ShapeDtyp...  144 us

profile of v5, /device:TPU:33, one launch (start us, length us, event | category | flops | bytes accessed | tf_op | source)
XLA Modules:
  0.0 145.4 jit_solution(3334206893691012899)
XLA Ops:
  0.0 143.5 %shard_map.163 = bf16[1024,256]{1,0:T(8,128)(2,1)} custom-call(bf16[1024,256]{1,0:T(8,128)(2,1)} %bitcast.7, f32[1,2048]{1,0:T(1,128)} %bitcast.10, f32[128,128]{1,0:T(8,128)} %in_m.1, f32[1,128]{1,0:T(1,128)} %in_s.1, bf16[1,128,128]{2,1,0:T(8,128)(2,1)} %pool_m.1, f32[1,128]{1,0:T(1,128)} %pool_s.1, f32[128,128]{1,0:T(8,128)} %out_m.1, f32[1,128]{1,0:T(1,128)} %out_s.1, ...), custom_call_target="tpu_custom_call" | custom-call | tf_op jit(solution)/shard_map/pallas_call | solution.py:705
  143.6 1.9 %copy.19 = bf16[1,1024,256]{2,1,0:T(8,128)(2,1)} copy(bf16[1,1024,256]{2,1,0:T(8,128)(2,1)} %bitcast.6) | data formatting | bytes 1048576
